TPU v7x, 512 devices: a whole 4x4x16 slice. The times are simulated.
512 devices in a mesh: ep: 32 (over z, core), tp: 16 (over y, x).
Axes of the slice: x: 4, y: 4, z: 16, core: 2. Of those that a mesh axis runs over, the one named last changes fastest.
Arguments:
- tokens: bfloat16 [2048, 2048], P('ep', 'tp'), may hold values from -20 to 20
- state: float32 [2048, 16, 64, 64], P('ep', 'tp'), may hold values from -1.5 to 1.5
- attn_gain: float32 [2048], replicated, may hold values from 0.1 to 1.9
- ffn_gain: float32 [2048], replicated, may hold values from 0.1 to 1.9
- w_query: bfloat16 [2048, 1024], P(None, 'tp'), may hold values from -0.125 to 0.125
- w_key: bfloat16 [2048, 1024], P(None, 'tp'), may hold values from -0.125 to 0.125
- w_value: bfloat16 [2048, 1024], P(None, 'tp'), may hold values from -0.125 to 0.125
- w_output_gate: bfloat16 [2048, 1024], P(None, 'tp'), may hold values from -0.125 to 0.125
- w_decay: bfloat16 [2048, 16], replicated, may hold values from -0.125 to 0.125
- w_beta: bfloat16 [2048, 16], replicated, may hold values from -0.125 to 0.125
- decay_rate: float32 [16], P('tp'), may hold values from 0.1 to 2
- decay_shift: float32 [16], P('tp'), may hold values from -2 to 1
- head_gain: float32 [64], replicated, may hold values from 0.1 to 1.9
- w_mix_out: bfloat16 [1024, 2048], P(None, 'tp'), may hold values from -0.1875 to 0.1875
- expert_ids: int32 [2048, 2], P('ep'), may hold values from 0 to 31, all different within a row; in each aligned block of 64 rows (0 to 63, 64 to 127, ...) at most 8 rows name the same one
- expert_weights: float32 [2048, 2], P('ep'), may hold values from 0.2 to 1
- w_gate: bfloat16 [32, 2048, 4096], P('ep', None, 'tp'), may hold values from -0.125 to 0.125
- w_up: bfloat16 [32, 2048, 4096], P('ep', None, 'tp'), may hold values from -0.125 to 0.125
- w_down: bfloat16 [32, 4096, 2048], P('ep', 'tp'), may hold values from -0.09375 to 0.09375
Outputs:
- layer_out: bfloat16 [2048, 2048], P('ep', 'tp')
- new_state: float32 [2048, 16, 64, 64], P('ep', 'tp')
Inputs may be any that keep to these rules, and one draw needn't show every extreme that they name: `expert_ids`: each row names 2 different experts; within the rows of one index of ep (aligned blocks of 64 rows) no expert is named by more than 8 rows, and in some blocks one expert is named by exactly 8 rows.
All inputs are finite; a program needn't handle non-finite values.
Results may differ from a plain program's by a relative error of at most 0.013.
Values may be sent and summed in bfloat16 or wider, within the bound.
No kernel may reach another device: no remote copies, remote signals or barrier semaphores. Data moves between devices by JAX's collectives and lax.ppermute only.
A program may use at most 64 MiB of HBM per device.

v0:
```python
import jax
import jax.numpy as jnp
from jax import lax
from jax.sharding import PartitionSpec as P

EPS = 1e-06


def laid_out(blocks, dim):
    dims = list(blocks.shape[1:])
    dims[dim] *= blocks.shape[0]
    return jnp.moveaxis(blocks, 0, dim).reshape(dims)


def from_everyone(shard, axis):
    devices = lax.axis_size(axis)
    return lax.all_to_all(
        jnp.broadcast_to(shard[None], (devices, *shard.shape)), axis, 0, 0, tiled=True
    )


def gathered_copies(shard, axis, dim):
    return laid_out(from_everyone(shard, axis), dim)


def over_copies(shard, axis):
    everything = from_everyone(shard, axis)
    return jnp.sum(everything, axis=0)


def in_blocks(shard, dim, devices):
    before, after = (shard.shape[:dim], shard.shape[dim + 1 :])
    return jnp.moveaxis(shard.reshape(*before, devices, -1, *after), dim, 0)


def sent_and_summed(shard, axis, dim):
    devices = lax.axis_size(axis)
    blocks = lax.all_to_all(in_blocks(shard, dim, devices), axis, 0, 0, tiled=True)
    return jnp.sum(blocks.astype(jnp.float32), axis=0)


def unit_norm(values):
    return values * lax.rsqrt(jnp.sum(values * values, axis=-1, keepdims=True) + EPS)


def stored(values):
    return lax.optimization_barrier(values.astype(jnp.bfloat16)).astype(jnp.float32)


def shards(
    tokens,
    state,
    attn_gain,
    ffn_gain,
    w_query,
    w_key,
    w_value,
    w_output_gate,
    w_decay,
    w_beta,
    decay_rate,
    decay_shift,
    head_gain,
    w_mix_out,
    expert_ids,
    expert_weights,
    w_gate,
    w_up,
    w_down,
):
    groups = lax.axis_size("ep")
    seq_count = tokens.shape[0]
    own_width = tokens.shape[1]
    model_width = ffn_gain.shape[0]
    head_dim = head_gain.shape[0]
    heads_here = decay_rate.shape[0]
    top_count = expert_ids.shape[1]
    local_experts = w_gate.shape[0]
    expert_total = local_experts * groups
    capacity = max(2, 2 * seq_count * top_count // expert_total)
    whole_rows = gathered_copies(tokens, "tp", 1)
    whole_f32 = whole_rows.astype(jnp.float32)
    normed = (
        whole_f32
        * lax.rsqrt(jnp.mean(whole_f32 * whole_f32, axis=1, keepdims=True) + EPS)
        * attn_gain
    ).astype(jnp.bfloat16)

    def project(weight):
        return jnp.dot(normed, weight, preferred_element_type=jnp.float32)

    def by_head(values):
        return values.reshape(seq_count, heads_here, head_dim)

    first_head = lax.axis_index("tp") * heads_here
    decay_cols = lax.dynamic_slice_in_dim(w_decay, first_head, heads_here, 1)
    beta_cols = lax.dynamic_slice_in_dim(w_beta, first_head, heads_here, 1)
    query_proj = stored(project(w_query))
    key_proj = stored(project(w_key))
    value_proj = stored(project(w_value))
    gate_proj = stored(project(w_output_gate))
    keep_rate = jnp.exp(-decay_rate * jax.nn.softplus(project(decay_cols) + decay_shift))
    beta_gate = jax.nn.sigmoid(project(beta_cols))
    query_head = unit_norm(jax.nn.silu(by_head(query_proj))) * head_dim ** (-0.5)
    key_head = unit_norm(jax.nn.silu(by_head(key_proj)))
    value_head = jax.nn.silu(by_head(value_proj))
    decayed = keep_rate[:, :, None, None] * state
    recalled = jnp.einsum("thd,thde->the", key_head, decayed, precision=lax.Precision.HIGHEST)
    correction = beta_gate[:, :, None] * (value_head - recalled)
    new_state = decayed + key_head[:, :, :, None] * correction[:, :, None, :]
    reading = jnp.einsum("thd,thde->the", query_head, new_state, precision=lax.Precision.HIGHEST)
    reading_scale = lax.rsqrt(jnp.mean(reading * reading, axis=-1, keepdims=True) + EPS)
    head_out = (reading * reading_scale * head_gain * jax.nn.silu(by_head(gate_proj))).astype(
        jnp.bfloat16
    )
    head_out = head_out.reshape(seq_count, heads_here * head_dim)
    mixed = jnp.dot(
        gathered_copies(head_out, "tp", 1), w_mix_out, preferred_element_type=jnp.float32
    )
    residual = (tokens.astype(jnp.float32) + mixed).astype(jnp.bfloat16)
    residual_f32 = residual.astype(jnp.float32)
    pair_count = seq_count * top_count
    flat_ids = expert_ids.reshape(pair_count)
    one_hot = (flat_ids[:, None] == jnp.arange(expert_total, dtype=jnp.int32)[None, :]).astype(
        jnp.int32
    )
    pair_index = jnp.arange(pair_count, dtype=jnp.int32)
    lower_mask = (pair_index[:, None] > pair_index[None, :]).astype(jnp.int32)
    earlier = jnp.dot(lower_mask, one_hot)
    slot_rank = jnp.sum(earlier * one_hot, axis=1)
    slot_of = flat_ids * capacity + slot_rank
    slot_count = expert_total * capacity
    slot_hit = jnp.arange(slot_count, dtype=jnp.int32)[:, None] == slot_of[None, :]
    dispatch = slot_hit.astype(jnp.bfloat16)
    dispatch_tokens = jnp.any(slot_hit.reshape(slot_count, seq_count, top_count), axis=2).astype(
        jnp.bfloat16
    )
    own_gain = lax.dynamic_slice_in_dim(ffn_gain, lax.axis_index("tp") * own_width, own_width, 0)
    square_total = over_copies(jnp.sum(residual_f32 * residual_f32, axis=1), "tp")
    row_scale = lax.rsqrt(square_total / model_width + EPS)
    normed_ffn = (residual_f32 * row_scale[:, None] * own_gain).astype(jnp.bfloat16)
    outgoing = jnp.dot(dispatch_tokens, normed_ffn, preferred_element_type=jnp.float32).astype(
        jnp.bfloat16
    )
    arrived = lax.all_to_all(outgoing, "ep", split_axis=0, concat_axis=0, tiled=True)
    segment = gathered_copies(arrived, "tp", 1)
    blocks = segment.reshape(groups, local_experts, capacity, segment.shape[1])
    gate_part = jnp.einsum("secd,edf->secf", blocks, w_gate, preferred_element_type=jnp.float32)
    up_part = jnp.einsum("secd,edf->secf", blocks, w_up, preferred_element_type=jnp.float32)
    expert_hidden = (jax.nn.silu(gate_part) * up_part).astype(jnp.bfloat16)
    partial_value = jnp.einsum(
        "secf,efd->secd", expert_hidden, w_down, preferred_element_type=jnp.float32
    )
    partial_value = partial_value.astype(jnp.bfloat16).reshape(
        groups * local_experts * capacity, model_width
    )
    summed = sent_and_summed(
        partial_value.astype(jnp.float32).astype(jnp.bfloat16), "tp", 1
    ).astype(jnp.bfloat16)
    returned = lax.all_to_all(summed, "ep", split_axis=0, concat_axis=0, tiled=True)
    pair_rows = jnp.einsum("sp,sd->pd", dispatch, returned, preferred_element_type=jnp.float32)
    weighted = jnp.sum(
        pair_rows.reshape(seq_count, top_count, own_width) * expert_weights[:, :, None], axis=1
    )
    layer_out = (residual_f32 + weighted).astype(jnp.bfloat16)
    return (layer_out, new_state)


def solution(mesh):
    in_specs = (
        P("ep", "tp"),
        P("ep", "tp", None, None),
        P(),
        P(),
        P(None, "tp"),
        P(None, "tp"),
        P(None, "tp"),
        P(None, "tp"),
        P(),
        P(),
        P("tp"),
        P("tp"),
        P(),
        P(None, "tp"),
        P("ep", None),
        P("ep", None),
        P("ep", None, "tp"),
        P("ep", None, "tp"),
        P("ep", "tp", None),
    )
    out_specs = (P("ep", "tp"), P("ep", "tp", None, None))
    return jax.shard_map(shards, mesh=mesh, in_specs=in_specs, out_specs=out_specs, check_vma=False)
```

profile of v0, /device:TPU:1, one launch (start us, length us, event | category | flops | bytes accessed | tf_op | source)
XLA Modules:
  0.0 149.1 jit_solution(3237636195357086897)
XLA Ops:
  0.7 1.6 %broadcast_in_dim.10 = bf16[16,64,128]{2,1,0:T(8,128)(2,1)} broadcast(bf16[64,128]{1,0:T(8,128)(2,1)} %param.19), dimensions={1,2} | broadcast | bytes 278528 | tf_op jit(solution)/shard_map/broadcast_in_dim | solution.py:18
  2.3 7.6 %all-to-all-start = ((bf16[16,64,128]{2,1,0:T(8,128)(2,1)}), bf16[16,64,128]{2,1,0:T(8,128)(2,1)S(1)}, u32[]{:S(2)}, u32[]{:S(2)}) async-start(bf16[16,64,128]{2,1,0:T(8,128)(2,1)} %broadcast_in_dim.10), calls=%async_computation | async-start | bytes 524288 | tf_op jit(solution)/shard_map/all_to_all | solution.py:17
  11.2 0.8 copy.61
  12.5 5.1 %all-to-all-done = bf16[16,64,128]{2,1,0:T(8,128)(2,1)S(1)} async-done(((bf16[16,64,128]{2,1,0:T(8,128)(2,1)}), bf16[16,64,128]{2,1,0:T(8,128)(2,1)S(1)}, u32[]{:S(2)}, u32[]{:S(2)}) %all-to-all-start) | async-done | bytes 262176 | tf_op jit(solution)/shard_map/all_to_all | solution.py:17
  17.7 0.8 fusion.29
  18.6 1.2 convolution_convert_fusion.4
  20.0 1.2 convolution_convert_fusion.3
  21.1 1.0 fusion.70
  22.2 1.9 %fusion.2 = f32[64,1,64]{2,1,0:T(1,128)S(1)} fusion(f32[64,64,1]{1,2,0:T(1,128)S(1)} %bitcast.147, f32[64,1,64,64]{3,2,1,0:T(8,128)S(1)} %copy-done.1, f32[64]{0:T(128)S(1)} %fusion.70), kind=kOutput, calls=%fused_computation.3 | convolution fusion | flops 3407872 | bytes 1081600 | tf_op jit(solution)/shard_map/thd,thde->the/dot_general | solution.py:108
  24.0 1.0 fusion.17
  25.1 0.8 multiply_add_fusion
  26.6 0.9 copy-done.2
  27.4 1.9 %fusion = f32[64,1,64]{2,1,0:T(1,128)S(1)} fusion(f32[64,64,1]{1,2,0:T(1,128)S(1)} %bitcast.152, f32[64,1,64,64]{3,2,1,0:T(8,128)S(1)} %multiply_add_fusion), kind=kOutput, calls=%fused_computation.1 | convolution fusion | flops 3145728 | bytes 1081344 | tf_op jit(solution)/shard_map/thd,thde->the/dot_general | solution.py:111
  29.8 0.9 reshape.298
  30.7 3.5 %all-to-all-start.1 = ((bf16[16,2,2048]{2,1,0:T(2,128)(2,1)}), bf16[16,2,2048]{2,1,0:T(2,128)(2,1)S(1)}, u32[]{:S(2)}, u32[]{:S(2)}) async-start(bf16[16,2,2048]{2,1,0:T(2,128)(2,1)} %reshape.298), calls=%async_computation.1 | async-start | bytes 262144 | tf_op jit(solution)/shard_map/all_to_all | solution.py:17
  34.2 6.8 %all-to-all-done.1 = bf16[16,2,2048]{2,1,0:T(2,128)(2,1)S(1)} async-done(((bf16[16,2,2048]{2,1,0:T(2,128)(2,1)}), bf16[16,2,2048]{2,1,0:T(2,128)(2,1)S(1)}, u32[]{:S(2)}, u32[]{:S(2)}) %all-to-all-start.1) | async-done | bytes 131104 | tf_op jit(solution)/shard_map/all_to_all | solution.py:17
  41.6 0.3 multiply_reduce_fusion
  41.9 0.6 broadcast_in_dim.12
  42.5 3.5 %all-to-all-start.2 = ((f32[16,1,64]{2,1,0:T(1,128)}), f32[16,1,64]{2,1,0:T(1,128)S(1)}, u32[]{:S(2)}, u32[]{:S(2)}) async-start(f32[16,1,64]{2,1,0:T(1,128)} %broadcast_in_dim.12), calls=%async_computation.2 | async-start | bytes 16384 | tf_op jit(solution)/shard_map/all_to_all | solution.py:17
  46.1 0.8 dynamic_slice.11
  46.8 5.4 %all-to-all-done.2 = f32[16,1,64]{2,1,0:T(1,128)S(1)} async-done(((f32[16,1,64]{2,1,0:T(1,128)}), f32[16,1,64]{2,1,0:T(1,128)S(1)}, u32[]{:S(2)}, u32[]{:S(2)}) %all-to-all-start.2) | async-done | bytes 4128 | tf_op jit(solution)/shard_map/all_to_all | solution.py:17
  52.6 32.3 %all_to_all.47 = bf16[32,8,128]{2,1,0:T(8,128)(2,1)S(1)} all-to-all(bf16[32,8,128]{2,1,0:T(8,128)(2,1)S(1)} %fusion.9), channel_id=1, replica_groups=mesh['ep'=32,'tp'=16] {'ep'}, dimensions={0} | all-to-all | bytes 131072 | tf_op jit(solution)/shard_map/all_to_all | solution.py:145
  85.1 18.2 %all_to_all.48 = bf16[16,256,128]{2,1,0:T(8,128)(2,1)S(1)} all-to-all(bf16[16,256,128]{2,1,0:T(8,128)(2,1)S(1)} %broadcast_in_dim.14), channel_id=1, replica_groups=mesh['ep'=32,'tp'=16] {'tp'}, dimensions={0} | all-to-all | bytes 2097152 | tf_op jit(solution)/shard_map/all_to_all | solution.py:17
  103.3 0.7 copy.64
  104.0 0.5 reshape.277
  104.5 1.7 %convolution_bitcast_fusion.1 = f32[32,1,8,256]{3,2,0,1:T(8,128)S(1)} fusion(bf16[32,8,2048]{2,1,0:T(8,128)(2,1)S(1)} %reshape.277, bf16[1,2048,256]{2,1,0:T(8,128)(2,1)} %param.35), kind=kOutput, calls=%fused_computation.10 | convolution fusion | flops 268435456 | bytes 2359296 | tf_op jit(solution)/shard_map/secd,edf->secf/dot_general | solution.py:148
  106.2 2.5 %fusion.5 = bf16[32,8,16,128]{3,1,2,0:T(8,128)(2,1)S(1)} fusion(bf16[1,256,2048]{2,1,0:T(8,128)(2,1)S(1)} %copy-done, bf16[32,8,2048]{2,1,0:T(8,128)(2,1)S(1)} %reshape.277, bf16[1,2048,256]{2,1,0:T(8,128)(2,1)} %param.36, f32[32,1,8,256]{3,2,0,1:T(8,128)S(1)} %convolution_bitcast_fusion.1), kind=kOutput, calls=%fused_computation.7 | convolution fusion | flops 537788416 | bytes 4456448 | tf_op jit(solution)/shard_map/secf,efd->secd/dot_general | solution.py:151
  109.2 16.7 %all_to_all.49 = bf16[16,256,128]{2,1,0:T(8,128)(2,1)S(1)} all-to-all(bf16[16,256,128]{2,1,0:T(8,128)(2,1)S(1)} %bitcast.145), channel_id=1, replica_groups=mesh['ep'=32,'tp'=16] {'tp'}, dimensions={0} | all-to-all | bytes 2097152 | tf_op jit(solution)/shard_map/all_to_all | solution.py:38
  125.9 0.8 reduce_sum.94
  126.7 8.6 %all-to-all-start.6 = ((bf16[32,8,128]{2,1,0:T(8,128)(2,1)}), bf16[32,8,128]{2,1,0:T(8,128)(2,1)S(1)}, u32[]{:S(2)}, u32[]{:S(2)}) async-start(bf16[32,8,128]{2,1,0:T(8,128)(2,1)} %bitcast.41), calls=%async_computation.6 | async-start | bytes 131072 | tf_op jit(solution)/shard_map/all_to_all | solution.py:160
  135.5 12.9 %all-to-all-done.6 = bf16[32,8,128]{2,1,0:T(8,128)(2,1)S(1)} async-done(((bf16[32,8,128]{2,1,0:T(8,128)(2,1)}), bf16[32,8,128]{2,1,0:T(8,128)(2,1)S(1)}, u32[]{:S(2)}, u32[]{:S(2)}) %all-to-all-start.6) | async-done | bytes 65568 | tf_op jit(solution)/shard_map/all_to_all | solution.py:160
  148.5 0.6 add_convert_fusion
  (55 shorter events, 4.0 us)
Async XLA Ops:
  0.6 105.5 %copy-start = (bf16[1,256,2048]{2,1,0:T(8,128)(2,1)S(1)}, bf16[1,256,2048]{2,1,0:T(8,128)(2,1)}, u32[]{:S(2)}) copy-start(bf16[1,256,2048]{2,1,0:T(8,128)(2,1)} %param.37) | copy-start | bytes 3145732
  0.6 20.5 %copy-start.7 = (f32[2048]{0:T(1024)S(1)}, f32[2048]{0:T(1024)}, u32[]{:S(2)}) copy-start(f32[2048]{0:T(1024)} %param.21) | copy-start | bytes 24580
  0.7 21.5 %copy-start.1 = (f32[64,1,64,64]{3,2,1,0:T(8,128)S(1)}, f32[64,1,64,64]{3,2,1,0:T(8,128)}, u32[]{:S(2)}) copy-start(f32[64,1,64,64]{3,2,1,0:T(8,128)} %param.20) | copy-start | bytes 3145732
  2.3 15.3 %all-to-all-start = ((bf16[16,64,128]{2,1,0:T(8,128)(2,1)}), bf16[16,64,128]{2,1,0:T(8,128)(2,1)S(1)}, u32[]{:S(2)}, u32[]{:S(2)}) async-start(bf16[16,64,128]{2,1,0:T(8,128)(2,1)} %broadcast_in_dim.10), calls=%async_computation | async-start | bytes 524288 | tf_op jit(solution)/shard_map/all_to_all | solution.py:17
  25.1 1.0 copy-start.3
  26.1 1.3 copy-start.2
  26.1 3.3 %copy-start.4 = (bf16[2048,64]{0,1:T(8,128)(2,1)S(1)}, bf16[2048,64]{0,1:T(8,128)(2,1)}, u32[]{:S(2)}) copy-start(bf16[2048,64]{0,1:T(8,128)(2,1)} %param.26) | copy-start | bytes 786436
  26.1 3.5 %copy-start.9 = (f32[64]{0:T(128)S(1)}, f32[64]{0:T(128)}, u32[]{:S(2)}) copy-start(f32[64]{0:T(128)} %param.31) | copy-start | bytes 772
  26.1 8.1 %copy-start.8 = (s32[64,2]{0,1:T(2,128)S(1)}, s32[64,2]{0,1:T(2,128)}, u32[]{:S(2)}) copy-start(s32[64,2]{0,1:T(2,128)} %param.33) | copy-start | bytes 1540
  27.4 14.2 %copy-start.5 = (bf16[1024,128]{1,0:T(8,128)(2,1)S(1)}, bf16[1024,128]{1,0:T(8,128)(2,1)}, u32[]{:S(2)}) copy-start(bf16[1024,128]{1,0:T(8,128)(2,1)} %param.32) | copy-start | bytes 786436
  27.4 14.2 %copy-start.6 = (bf16[64,128]{1,0:T(8,128)(2,1)S(1)}, bf16[64,128]{1,0:T(8,128)(2,1)}, u32[]{:S(2)}) copy-start(bf16[64,128]{1,0:T(8,128)(2,1)} %param.19) | copy-start | bytes 49156
  30.7 10.3 %all-to-all-start.1 = ((bf16[16,2,2048]{2,1,0:T(2,128)(2,1)}), bf16[16,2,2048]{2,1,0:T(2,128)(2,1)S(1)}, u32[]{:S(2)}, u32[]{:S(2)}) async-start(bf16[16,2,2048]{2,1,0:T(2,128)(2,1)} %reshape.298), calls=%async_computation.1 | async-start | bytes 262144 | tf_op jit(solution)/shard_map/all_to_all | solution.py:17
  42.5 9.8 %all-to-all-start.2 = ((f32[16,1,64]{2,1,0:T(1,128)}), f32[16,1,64]{2,1,0:T(1,128)S(1)}, u32[]{:S(2)}, u32[]{:S(2)}) async-start(f32[16,1,64]{2,1,0:T(1,128)} %broadcast_in_dim.12), calls=%async_computation.2 | async-start | bytes 16384 | tf_op jit(solution)/shard_map/all_to_all | solution.py:17
  109.2 39.1 %copy-start.10 = (f32[64,2]{0,1:T(2,128)S(1)}, f32[64,2]{0,1:T(2,128)}, u32[]{:S(2)}) copy-start(f32[64,2]{0,1:T(2,128)} %param.34) | copy-start | bytes 1540
  126.7 21.7 %all-to-all-start.6 = ((bf16[32,8,128]{2,1,0:T(8,128)(2,1)}), bf16[32,8,128]{2,1,0:T(8,128)(2,1)S(1)}, u32[]{:S(2)}, u32[]{:S(2)}) async-start(bf16[32,8,128]{2,1,0:T(8,128)(2,1)} %bitcast.41), calls=%async_computation.6 | async-start | bytes 131072 | tf_op jit(solution)/shard_map/all_to_all | solution.py:160
where the time goes:
time: 150 us; the launch traced here: 149 us
  blocking collectives  67.2 us (45%)
  waiting for transfers between devices  30.2 us (20%)
  starting transfers between devices  23.2 us (15%)
  matrix products  13.5 us (9%)
  local copies, waits for them, and re-layouts  8.57 us (6%)
  other arithmetic  4.13 us (3%)
  between operations  2.29 us (2%)
    all_to_all x1, blocking collectives, shards(): lax.all_to_all(outgoing, 'ep', split_axis=0, concat_axis=0, tiled=True)  32.3 us
    all_to_all x1, blocking collectives, from_everyone(): lax.all_to_all(jnp.broadcast_to(shard[None], (devices, *shard.shape)), ax...  18.2 us
    all_to_all x3, waiting for transfers between devices, from_everyone(): lax.all_to_all(jnp.broadcast_to(shard[None], (devices, *shard.shape)), ax...  17.3 us
    all_to_all x1, blocking collectives, sent_and_summed(): lax.all_to_all(in_blocks(shard, dim, devices), axis, 0, 0, tiled=True)  16.7 us
    all_to_all x3, starting transfers between devices, from_everyone(): lax.all_to_all(jnp.broadcast_to(shard[None], (devices, *shard.shape)), ax...  14.6 us
    all_to_all x1, waiting for transfers between devices, shards(): lax.all_to_all(summed, 'ep', split_axis=0, concat_axis=0, tiled=True)  12.9 us
    all_to_all x1, starting transfers between devices, shards(): lax.all_to_all(summed, 'ep', split_axis=0, concat_axis=0, tiled=True)  8.63 us
    dot_general x6, matrix products, project(): return jnp.dot(normed, weight, preferred_element_type=jnp.float32)  4.8 us
  transfers between devices with their start and end apart: 4, of which 4 were waited for; matrix products, arithmetic and copies ran while one was open for 2% of the time, Pallas kernels for 0%

commit v1 on v0

v1 whole, which is shorter than its diff:
```python
import jax
import jax.numpy as jnp
from jax import lax
from jax.sharding import Mesh, PartitionSpec as P

EPS = 1e-06
TP = ("y", "x")
PLANE = ("c", "y", "x")


def exchanged(blocks, axes):
    return lax.all_to_all(blocks, axes, 0, 0, tiled=True)


def to_everyone(shard, axes):
    count = lax.axis_size(axes)
    return exchanged(jnp.broadcast_to(shard[None], (count, *shard.shape)), axes)


def unit_norm(values):
    return values * lax.rsqrt(jnp.sum(values * values, axis=-1, keepdims=True) + EPS)


def stored(values):
    return lax.optimization_barrier(values.astype(jnp.bfloat16)).astype(jnp.float32)


def row_norm(values, gain):
    scale = lax.rsqrt(jnp.mean(values * values, axis=1, keepdims=True) + EPS)
    return (values * scale * gain).astype(jnp.bfloat16)


def side_by_side(blocks):
    return jnp.moveaxis(blocks, 0, 1).reshape(blocks.shape[1], -1)


def shards(
    tokens,
    state,
    attn_gain,
    ffn_gain,
    w_query,
    w_key,
    w_value,
    w_output_gate,
    w_decay,
    w_beta,
    decay_rate,
    decay_shift,
    head_gain,
    w_mix_out,
    expert_ids,
    expert_weights,
    w_gate,
    w_up,
    w_down,
):
    planes = lax.axis_size("z")
    cores = lax.axis_size("c")
    tp_size = lax.axis_size(TP)
    seq_count = tokens.shape[0]
    own_width = tokens.shape[1]
    head_dim = head_gain.shape[0]
    top_count = expert_ids.shape[1]
    expert_total = planes * cores
    capacity = 2 * seq_count * top_count // expert_total

    experts = jnp.arange(expert_total, dtype=jnp.int32)
    one_hot = (expert_ids[:, :, None] == experts).astype(jnp.float32)
    position = jnp.arange(seq_count, dtype=jnp.int32)
    before = (position[:, None] > position[None, :]).astype(jnp.float32)
    earlier = jnp.dot(before, jnp.sum(one_hot, axis=1))
    slots = jnp.arange(expert_total * capacity, dtype=jnp.int32)
    hits = []
    for choice in range(top_count):
        rank = jnp.sum(earlier * one_hot[:, choice], axis=1).astype(jnp.int32)
        slot = expert_ids[:, choice] * capacity + rank
        hits.append(slot[:, None] == slots[None, :])
    pick = (hits[0] | hits[1]).astype(jnp.bfloat16)
    hits = [hit.astype(jnp.bfloat16) for hit in hits]

    whole = side_by_side(to_everyone(tokens, TP)).astype(jnp.float32)
    normed = row_norm(whole, attn_gain)

    def project(weight):
        return jnp.dot(normed, weight, preferred_element_type=jnp.float32)

    head = lax.axis_index(TP)
    decay_col = lax.dynamic_slice_in_dim(w_decay, head, 1, 1)
    beta_col = lax.dynamic_slice_in_dim(w_beta, head, 1, 1)
    query_proj = stored(project(w_query))
    key_proj = stored(project(w_key))
    value_proj = stored(project(w_value))
    gate_proj = stored(project(w_output_gate))
    keep_rate = jnp.exp(-decay_rate * jax.nn.softplus(project(decay_col) + decay_shift))
    beta_gate = jax.nn.sigmoid(project(beta_col))
    query_head = unit_norm(jax.nn.silu(query_proj)) * head_dim ** (-0.5)
    key_head = unit_norm(jax.nn.silu(key_proj))
    value_head = jax.nn.silu(value_proj)
    decayed = keep_rate[:, :, None] * state[:, 0]
    recalled = jnp.einsum("td,tde->te", key_head, decayed, precision=lax.Precision.HIGHEST)
    correction = beta_gate * (value_head - recalled)
    new_state = decayed + key_head[:, :, None] * correction[:, None, :]
    reading = jnp.einsum("td,tde->te", query_head, new_state, precision=lax.Precision.HIGHEST)
    reading_scale = lax.rsqrt(jnp.mean(reading * reading, axis=-1, keepdims=True) + EPS)
    head_out = (reading * reading_scale * head_gain * jax.nn.silu(gate_proj)).astype(jnp.bfloat16)

    all_heads = side_by_side(to_everyone(head_out, TP))
    mixed = jnp.dot(all_heads, w_mix_out, preferred_element_type=jnp.float32)
    residual = (tokens.astype(jnp.float32) + mixed).astype(jnp.bfloat16)

    outgoing = lax.dot_general(
        pick, residual, (((0,), (0,)), ((), ())), preferred_element_type=jnp.float32
    ).astype(jnp.bfloat16)
    along_z = exchanged(outgoing.reshape(planes, cores * capacity, own_width), "z")
    per_core = jnp.moveaxis(along_z.reshape(planes, cores, capacity, own_width), 1, 0)
    half_rows = planes * capacity
    spread = jnp.broadcast_to(
        per_core.reshape(cores, 1, half_rows, own_width), (cores, tp_size, half_rows, own_width)
    )
    arrived = exchanged(spread.reshape(cores * tp_size, half_rows, own_width), PLANE)
    arrived = arrived.reshape(cores, tp_size, half_rows, own_width)
    rows = jnp.moveaxis(arrived, 1, 2).reshape(cores * half_rows, tp_size * own_width)
    rows = row_norm(rows.astype(jnp.float32), ffn_gain)

    gate_part = jnp.dot(rows, w_gate[0], preferred_element_type=jnp.float32)
    up_part = jnp.dot(rows, w_up[0], preferred_element_type=jnp.float32)
    hidden = (jax.nn.silu(gate_part) * up_part).astype(jnp.bfloat16)
    partial_value = jnp.dot(hidden, w_down[0], preferred_element_type=jnp.float32)
    partial_value = partial_value.astype(jnp.bfloat16)
    parts = jnp.moveaxis(partial_value.reshape(cores, half_rows, tp_size, own_width), 2, 1)
    parts = exchanged(parts.reshape(cores * tp_size, half_rows, own_width), PLANE)
    parts = parts.reshape(cores, tp_size, half_rows, own_width).astype(jnp.float32)
    summed = jnp.sum(parts, axis=1).astype(jnp.bfloat16)
    back = jnp.moveaxis(summed.reshape(cores, planes, capacity, own_width), 0, 1)
    returned = exchanged(back.reshape(planes, cores * capacity, own_width), "z")
    returned = returned.reshape(expert_total * capacity, own_width)

    weighted = 0.0
    for choice in range(top_count):
        pair = jnp.dot(hits[choice], returned, preferred_element_type=jnp.float32)
        weighted += pair * expert_weights[:, choice : choice + 1]
    layer_out = (residual.astype(jnp.float32) + weighted).astype(jnp.bfloat16)
    return (layer_out, new_state[:, None])


def solution(mesh):
    axes = Mesh(mesh.devices.reshape(16, 2, 4, 4), ("z", "c", "y", "x"))
    ep = ("z", "c")
    in_specs = (
        P(ep, TP),
        P(ep, TP, None, None),
        P(),
        P(),
        P(None, TP),
        P(None, TP),
        P(None, TP),
        P(None, TP),
        P(),
        P(),
        P(TP),
        P(TP),
        P(),
        P(None, TP),
        P(ep, None),
        P(ep, None),
        P(ep, None, TP),
        P(ep, None, TP),
        P(ep, TP, None),
    )
    out_specs = (P(ep, TP), P(ep, TP, None, None))
    return jax.shard_map(shards, mesh=axes, in_specs=in_specs, out_specs=out_specs, check_vma=False)
```

time: 150 us -> 148 us (0.987)
  blocking collectives: 67.2 us -> 50.7 us
  waiting for transfers between devices: 30.2 us -> 38.1 us
  matrix products: 13.5 us -> 17.3 us
  other arithmetic: 4.13 us -> 6.99 us
  local copies, waits for them, and re-layouts: 8.57 us -> 11 us
  starting transfers between devices: 23.2 us -> 21 us
    all_to_all x3 -> x2, blocking collectives: 67.2 us -> 50.7 us  [exchanged(): return lax.all_to_all(blocks, axes, 0, 0, tiled=True)]
    all_to_all x4, waiting for transfers between devices: 30.2 us -> 38.1 us  [exchanged(): return lax.all_to_all(blocks, axes, 0, 0, tiled=True)]
    dot_general x8 -> x9, matrix products: 8.7 us -> 11.6 us  [the longest x1 3.86 us: shards(): jnp.dot(hidden, w_down[0], preferred_element_type=jnp.float32)]
    reshape x3, local copies, waits for them, and re-layouts: 0.61 us -> 3.02 us  [the longest x1 1.24 us: shards(): partial_value.reshape(cores, half_rows, tp_size, own_width)]
    all_to_all x4, starting transfers between devices: 23.2 us -> 21 us  [exchanged(): return lax.all_to_all(blocks, axes, 0, 0, tiled=True)]
    reduce_sum x3 -> x4, other arithmetic: 0.94 us -> 2.5 us  [the longest x1 1.37 us: shards(): summed = jnp.sum(parts, axis=1).astype(jnp.bfloat16)]
    unnamed x26 -> x25, local copies, waits for them, and re-layouts: 3.12 us -> 4.48 us
where the time goes in v1:
time: 148 us; the launch traced here: 147 us
  blocking collectives  50.7 us (34%)
  waiting for transfers between devices  38.1 us (26%)
  starting transfers between devices  21 us (14%)
  matrix products  17.3 us (12%)
  local copies, waits for them, and re-layouts  11 us (7%)
  other arithmetic  6.99 us (5%)
  between operations  2.24 us (2%)
    all_to_all x2, blocking collectives, exchanged(): return lax.all_to_all(blocks, axes, 0, 0, tiled=True)  50.7 us
    all_to_all x4, waiting for transfers between devices, exchanged(): return lax.all_to_all(blocks, axes, 0, 0, tiled=True)  38.1 us
    all_to_all x4, starting transfers between devices, exchanged(): return lax.all_to_all(blocks, axes, 0, 0, tiled=True)  21 us
    dot_general x6, matrix products, project(): return jnp.dot(normed, weight, preferred_element_type=jnp.float32)  5.76 us
    unnamed x25, local copies, waits for them, and re-layouts  4.48 us
    dot_general x1, matrix products, shards(): jnp.dot(hidden, w_down[0], preferred_element_type=jnp.float32)  3.86 us
  transfers between devices with their start and end apart: 4, of which 4 were waited for; matrix products, arithmetic and copies ran while one was open for 2% of the time, Pallas kernels for 0%

profile of v1, /device:TPU:1, one launch (start us, length us, event | category | flops | bytes accessed | tf_op | source)
XLA Modules:
  0.0 147.3 jit_solution(15459666206254157575)
XLA Ops:
  0.7 1.6 %broadcast_in_dim.8 = bf16[16,64,128]{2,1,0:T(8,128)(2,1)} broadcast(bf16[64,128]{1,0:T(8,128)(2,1)} %param.19), dimensions={1,2} | broadcast | bytes 278528 | tf_op jit(solution)/shard_map/broadcast_in_dim | solution.py:17
  2.3 7.6 %all-to-all-start = ((bf16[16,64,128]{2,1,0:T(8,128)(2,1)}), bf16[16,64,128]{2,1,0:T(8,128)(2,1)S(1)}, u32[]{:S(2)}, u32[]{:S(2)}) async-start(bf16[16,64,128]{2,1,0:T(8,128)(2,1)} %broadcast_in_dim.8), calls=%async_computation | async-start | bytes 524288 | tf_op jit(solution)/shard_map/all_to_all | solution.py:12
  12.7 4.9 %all-to-all-done = bf16[16,64,128]{2,1,0:T(8,128)(2,1)S(1)} async-done(((bf16[16,64,128]{2,1,0:T(8,128)(2,1)}), bf16[16,64,128]{2,1,0:T(8,128)(2,1)S(1)}, u32[]{:S(2)}, u32[]{:S(2)}) %all-to-all-start) | async-done | bytes 262176 | tf_op jit(solution)/shard_map/all_to_all | solution.py:12
  17.7 0.8 fusion.39
  18.6 1.2 convolution_convert_fusion.4
  20.0 1.2 convolution_convert_fusion.3
  21.1 1.2 convolution_convert_fusion.5
  22.5 1.0 fusion.89
  23.6 1.8 %fusion.6 = f32[64,1,64]{2,1,0:T(1,128)S(1)} fusion(f32[64,64,1]{1,2,0:T(1,128)S(1)} %bitcast.168, f32[64,1,64,64]{3,2,1,0:T(8,128)S(1)} %copy-done.1, f32[64]{0:T(128)S(1)} %fusion.89), kind=kOutput, calls=%fused_computation.11 | convolution fusion | flops 3407872 | bytes 1081600 | tf_op jit(solution)/shard_map/td,tde->te/dot_general | solution.py:101
  25.4 1.0 fusion.16
  26.6 2.1 %fusion.3 = f32[64,1,64]{2,1,0:T(1,128)S(1)} fusion(f32[64,64,1]{1,2,0:T(1,128)S(1)} %bitcast.171, f32[64,1,64,64]{3,2,1,0:T(8,128)S(1)} %copy-done.1, f32[64,64]{1,0:T(8,128)S(1)} %fusion.63, f32[64,64]{1,0:T(8,128)S(1)} %broadcast_multiply_fusion, f32[64]{0:T(128)S(1)} %fusion.89), kind=kOutput, calls=%fused_computation.8 | convolution fusion | flops 3932160 | bytes 1114368 | tf_op jit(solution)/shard_map/td,tde->te/dot_general | solution.py:104
  29.2 0.9 reshape.206
  30.1 4.2 %all-to-all-start.1 = ((bf16[16,2,2048]{2,1,0:T(2,128)(2,1)}), bf16[16,2,2048]{2,1,0:T(2,128)(2,1)}, u32[]{:S(2)}, u32[]{:S(2)}) async-start(bf16[16,2,2048]{2,1,0:T(2,128)(2,1)} %reshape.206), calls=%async_computation.1 | async-start | bytes 262144 | tf_op jit(solution)/shard_map/all_to_all | solution.py:12
  34.3 6.8 %all-to-all-done.1 = bf16[16,2,2048]{2,1,0:T(2,128)(2,1)} async-done(((bf16[16,2,2048]{2,1,0:T(2,128)(2,1)}), bf16[16,2,2048]{2,1,0:T(2,128)(2,1)}, u32[]{:S(2)}, u32[]{:S(2)}) %all-to-all-start.1) | async-done | bytes 131104 | tf_op jit(solution)/shard_map/all_to_all | solution.py:12
  41.1 1.1 reshape.207
  42.2 0.9 copy.28
  43.1 1.1 reshape.184
  44.3 1.1 fusion.12
  45.7 26.1 %all_to_all.30 = bf16[16,16,128]{2,1,0:T(8,128)(2,1)S(1)} all-to-all(bf16[16,16,128]{2,1,0:T(8,128)(2,1)S(1)} %bitcast.175), channel_id=1, replica_groups=mesh['z'=16,'c'=2,'y'=4,'x'=4] {'z'}, dimensions={0} | all-to-all | bytes 131072 | tf_op jit(solution)/shard_map/all_to_all | solution.py:12
  72.1 24.5 %all_to_all.31 = bf16[32,128,128]{2,1,0:T(8,128)(2,1)S(1)} all-to-all(bf16[32,128,128]{2,1,0:T(8,128)(2,1)S(1)} %bitcast.163), channel_id=1, replica_groups=mesh['z'=16,'c'=2,'y'=4,'x'=4] {'c','y','x'}, dimensions={0} | all-to-all | bytes 2097152 | tf_op jit(solution)/shard_map/all_to_all | solution.py:12
  98.1 1.0 copy-done.2
  99.0 1.2 fusion.20
  100.2 3.9 %fusion.7 = bf16[32,8,16,128]{3,1,2,0:T(8,128)(2,1)} fusion(bf16[1,256,2048]{2,1,0:T(8,128)(2,1)S(1)} %copy-done, bf16[1,2048,256]{2,1,0:T(8,128)(2,1)} %param.36, bf16[32,8,16,128]{3,2,1,0:T(8,128)(2,1)} %bitcast.166, f32[256,256]{1,0:T(8,128)} %fusion.20), kind=kOutput, calls=%fused_computation.12 | convolution fusion | flops 537788416 | bytes 4456448 | tf_op jit(solution)/shard_map/dot_general | solution.py:129
  104.0 1.4 copy.40
  105.5 1.2 copy.31
  106.8 5.8 %all-to-all-start.4 = ((bf16[32,128,128]{2,1,0:T(8,128)(2,1)}), bf16[32,128,128]{2,1,0:T(8,128)(2,1)}, u32[]{:S(2)}, u32[]{:S(2)}) async-start(bf16[32,128,128]{2,1,0:T(8,128)(2,1)} %bitcast.162), calls=%async_computation.4 | async-start | bytes 2097152 | tf_op jit(solution)/shard_map/all_to_all | solution.py:12
  112.6 16.6 %all-to-all-done.4 = bf16[32,128,128]{2,1,0:T(8,128)(2,1)} async-done(((bf16[32,128,128]{2,1,0:T(8,128)(2,1)}), bf16[32,128,128]{2,1,0:T(8,128)(2,1)}, u32[]{:S(2)}, u32[]{:S(2)}) %all-to-all-start.4) | async-done | bytes 1048608 | tf_op jit(solution)/shard_map/all_to_all | solution.py:12
  129.2 1.4 bitcast_reduce_fusion
  131.2 3.5 %all-to-all-start.5 = ((bf16[16,16,128]{2,1,0:T(8,128)(2,1)}), bf16[16,16,128]{2,1,0:T(8,128)(2,1)S(1)}, u32[]{:S(2)}, u32[]{:S(2)}) async-start(bf16[16,16,128]{2,1,0:T(8,128)(2,1)} %copy_bitcast_fusion), calls=%async_computation.5 | async-start | bytes 131072 | tf_op jit(solution)/shard_map/all_to_all | solution.py:12
  134.7 1.8 %multiply_add_fusion = f32[64,1,64,64]{3,2,1,0:T(8,128)} fusion(f32[64,1,64,64]{3,2,1,0:T(8,128)S(1)} %copy-done.1, f32[64,64]{1,0:T(8,128)S(1)} %fusion.63, f32[64,64]{1,0:T(8,128)S(1)} %broadcast_multiply_fusion, f32[64]{0:T(128)S(1)} %fusion.89), kind=kLoop, calls=%fused_computation.7 | loop fusion | flops 786432 | bytes 2130176 | tf_op jit(solution)/shard_map/add | solution.py:103
  136.5 9.8 %all-to-all-done.5 = bf16[16,16,128]{2,1,0:T(8,128)(2,1)S(1)} async-done(((bf16[16,16,128]{2,1,0:T(8,128)(2,1)}), bf16[16,16,128]{2,1,0:T(8,128)(2,1)S(1)}, u32[]{:S(2)}, u32[]{:S(2)}) %all-to-all-start.5) | async-done | bytes 65568 | tf_op jit(solution)/shard_map/all_to_all | solution.py:12
  146.5 0.8 fusion.11
  (49 shorter events, 5.5 us)
Async XLA Ops:
  0.6 99.6 %copy-start = (bf16[1,256,2048]{2,1,0:T(8,128)(2,1)S(1)}, bf16[1,256,2048]{2,1,0:T(8,128)(2,1)}, u32[]{:S(2)}) copy-start(bf16[1,256,2048]{2,1,0:T(8,128)(2,1)} %param.37) | copy-start | bytes 3145732
  0.6 21.9 %copy-start.6 = (f32[2048]{0:T(1024)S(1)}, f32[2048]{0:T(1024)}, u32[]{:S(2)}) copy-start(f32[2048]{0:T(1024)} %param.21) | copy-start | bytes 24580
  0.7 22.9 %copy-start.1 = (f32[64,1,64,64]{3,2,1,0:T(8,128)S(1)}, f32[64,1,64,64]{3,2,1,0:T(8,128)}, u32[]{:S(2)}) copy-start(f32[64,1,64,64]{3,2,1,0:T(8,128)} %param.20) | copy-start | bytes 3145732
  2.3 15.3 %all-to-all-start = ((bf16[16,64,128]{2,1,0:T(8,128)(2,1)}), bf16[16,64,128]{2,1,0:T(8,128)(2,1)S(1)}, u32[]{:S(2)}, u32[]{:S(2)}) async-start(bf16[16,64,128]{2,1,0:T(8,128)(2,1)} %broadcast_in_dim.8), calls=%async_computation | async-start | bytes 524288 | tf_op jit(solution)/shard_map/all_to_all | solution.py:12
  23.6 5.3 %copy-start.3 = (bf16[2048,64]{0,1:T(8,128)(2,1)S(1)}, bf16[2048,64]{0,1:T(8,128)(2,1)}, u32[]{:S(2)}) copy-start(bf16[2048,64]{0,1:T(8,128)(2,1)} %param.26) | copy-start | bytes 786436
  25.4 3.6 %copy-start.9 = (f32[64]{0:T(128)S(1)}, f32[64]{0:T(128)}, u32[]{:S(2)}) copy-start(f32[64]{0:T(128)} %param.31) | copy-start | bytes 772
  26.5 7.8 %copy-start.5 = (s32[64,2]{0,1:T(2,128)S(1)}, s32[64,2]{0,1:T(2,128)}, u32[]{:S(2)}) copy-start(s32[64,2]{0,1:T(2,128)} %param.33) | copy-start | bytes 1540
  26.6 17.7 %copy-start.4 = (bf16[64,128]{1,0:T(8,128)(2,1)S(1)}, bf16[64,128]{1,0:T(8,128)(2,1)}, u32[]{:S(2)}) copy-start(bf16[64,128]{1,0:T(8,128)(2,1)} %param.19) | copy-start | bytes 49156
  30.1 11.0 %all-to-all-start.1 = ((bf16[16,2,2048]{2,1,0:T(2,128)(2,1)}), bf16[16,2,2048]{2,1,0:T(2,128)(2,1)}, u32[]{:S(2)}, u32[]{:S(2)}) async-start(bf16[16,2,2048]{2,1,0:T(2,128)(2,1)} %reshape.206), calls=%async_computation.1 | async-start | bytes 262144 | tf_op jit(solution)/shard_map/all_to_all | solution.py:12
  71.8 25.1 %copy-start.7 = (f32[2048]{0:T(1024)S(1)}, f32[2048]{0:T(1024)}, u32[]{:S(2)}) copy-start(f32[2048]{0:T(1024)} %param.22) | copy-start | bytes 24580
  96.9 2.1 %copy-start.10 = (bf16[1,2048,256]{2,1,0:T(8,128)(2,1)S(1)}, bf16[1,2048,256]{2,1,0:T(8,128)(2,1)}, u32[]{:S(2)}) copy-start(bf16[1,2048,256]{2,1,0:T(8,128)(2,1)} %param.35) | copy-start | bytes 3145732
  98.0 1.0 copy-start.2
  105.5 7.1 %copy-start.8 = (f32[64,2]{0,1:T(2,128)S(1)}, f32[64,2]{0,1:T(2,128)}, u32[]{:S(2)}) copy-start(f32[64,2]{0,1:T(2,128)} %param.34) | copy-start | bytes 1540
  106.8 22.4 %all-to-all-start.4 = ((bf16[32,128,128]{2,1,0:T(8,128)(2,1)}), bf16[32,128,128]{2,1,0:T(8,128)(2,1)}, u32[]{:S(2)}, u32[]{:S(2)}) async-start(bf16[32,128,128]{2,1,0:T(8,128)(2,1)} %bitcast.162), calls=%async_computation.4 | async-start | bytes 2097152 | tf_op jit(solution)/shard_map/all_to_all | solution.py:12
  131.2 15.1 %all-to-all-start.5 = ((bf16[16,16,128]{2,1,0:T(8,128)(2,1)}), bf16[16,16,128]{2,1,0:T(8,128)(2,1)S(1)}, u32[]{:S(2)}, u32[]{:S(2)}) async-start(bf16[16,16,128]{2,1,0:T(8,128)(2,1)} %copy_bitcast_fusion), calls=%async_computation.5 | async-start | bytes 131072 | tf_op jit(solution)/shard_map/all_to_all | solution.py:12

commit v2 on v1

v2 whole, which is shorter than its diff:
```python
import functools

import jax
import jax.numpy as jnp
from jax import lax
from jax.experimental import pallas as pl
from jax.experimental.pallas import tpu as pltpu
from jax.sharding import Mesh, PartitionSpec as P

EPS = 1e-06
TP = ("y", "x")
PLANE = ("c", "y", "x")
BF16 = jnp.bfloat16
F32 = jnp.float32
VMEM_LIMIT = 12 << 20


def exchanged(blocks, axes):
    return lax.all_to_all(blocks, axes, 0, 0, tiled=True)


def to_everyone(shard, axes):
    count = lax.axis_size(axes)
    return exchanged(jnp.broadcast_to(shard[None], (count, *shard.shape)), axes)


def silu(values):
    return values * (1.0 / (1.0 + jnp.exp(-values)))


def rounded(values):
    return values.astype(BF16).astype(F32)


def local_call(kernel, out_shapes, scratch, flops, *operands, scalars=()):
    vmem = pl.BlockSpec(memory_space=pltpu.VMEM)
    smem = pl.BlockSpec(memory_space=pltpu.SMEM)
    outs = [jax.ShapeDtypeStruct(shape, dtype) for shape, dtype in out_shapes]
    return pl.pallas_call(
        kernel,
        out_shape=outs,
        in_specs=[vmem] * len(operands) + [smem] * len(scalars),
        out_specs=[vmem] * len(outs),
        scratch_shapes=scratch,
        compiler_params=pltpu.CompilerParams(vmem_limit_bytes=VMEM_LIMIT),
        cost_estimate=pl.CostEstimate(flops=flops, bytes_accessed=1 << 20, transcendentals=0),
    )(*operands, *scalars)


def prepare_kernel(expert_total, capacity, ids, w_decay, w_beta, head, w_rates, slots):
    model_width = w_rates.shape[1]
    rows = []
    for weight in (w_decay, w_beta):
        values = weight[...].astype(F32)
        own = lax.broadcasted_iota(jnp.int32, values.shape, 0) == head[0]
        rows.append(jnp.sum(jnp.where(own, values, 0.0), axis=0, keepdims=True))
    row = lax.broadcasted_iota(jnp.int32, w_rates.shape, 0)
    w_rates[...] = jnp.where(row == 0, rows[0], jnp.where(row == 1, rows[1], 0.0)).astype(BF16)
    choices, seqs = ids.shape
    experts = lax.broadcasted_iota(jnp.int32, (expert_total, seqs), 0)
    chosen = [(ids[choice : choice + 1, :] == experts).astype(F32) for choice in range(choices)]
    source = lax.broadcasted_iota(jnp.int32, (seqs, seqs), 0)
    target = lax.broadcasted_iota(jnp.int32, (seqs, seqs), 1)
    before = (source < target).astype(F32).astype(BF16)
    earlier = jnp.dot((chosen[0] + chosen[1]).astype(BF16), before, preferred_element_type=F32)
    for choice in range(choices):
        rank = jnp.sum(earlier * chosen[choice], axis=0, keepdims=True).astype(jnp.int32)
        slots[choice : choice + 1, :] = ids[choice : choice + 1, :] * capacity + rank


def slot_hits(slots, slot_count):
    places = lax.broadcasted_iota(jnp.int32, (slot_count, slots.shape[1]), 0)
    return [(slots[choice : choice + 1, :] == places).astype(F32).astype(BF16) for choice in range(2)]


def lane_pair(left, right):
    shape = (left.shape[0], 128)
    lane = lax.broadcasted_iota(jnp.int32, shape, 1)
    return jnp.where(lane < 64, jnp.broadcast_to(left, shape), jnp.broadcast_to(right, shape))


def attend_kernel(tok, gain, wq, wk, wv, wg, w_rates, head_gain, state, rate, shift,
                  spread, corr_out, keep_out, key_out, normed, from_key, from_query):
    tiles, seqs, width = tok.shape
    head_dim = wq.shape[0]
    half = seqs // 2
    squares = jnp.zeros((seqs, width), F32)
    for tile in range(tiles):
        x = tok[tile].astype(F32)
        squares += x * x
    mean = jnp.sum(squares, axis=1, keepdims=True) / (tiles * width)
    scale = lax.rsqrt(mean + EPS)
    for tile in range(tiles):
        cols = slice(tile * width, (tile + 1) * width)
        normed[:, cols] = (tok[tile].astype(F32) * scale * gain[:, cols]).astype(BF16)
    rows = normed[...]
    dims = (((1,), (1,)), ((), ()))

    def project(weight):
        return lax.dot_general(rows, weight, dims, preferred_element_type=F32)

    def project_across(weight):
        return lax.dot_general(weight, rows, dims, preferred_element_type=F32)

    def unit(values, axis):
        return values * lax.rsqrt(jnp.sum(values * values, axis=axis, keepdims=True) + EPS)

    def packed(values):
        return jnp.concatenate([values[:half], values[half:]], axis=1)

    key_across = unit(silu(rounded(project_across(wk[...]))), 0)
    query_across = unit(silu(rounded(project_across(wq[...]))), 0) * head_dim ** (-0.5)
    for t in range(half):
        u = half + t
        block = jnp.concatenate([state[t], state[u]], axis=1)
        key_pair = lane_pair(key_across[:, t : t + 1], key_across[:, u : u + 1])
        query_pair = lane_pair(query_across[:, t : t + 1], query_across[:, u : u + 1])
        from_key[t : t + 1, :] = jnp.sum(key_pair * block, axis=0, keepdims=True)
        from_query[t : t + 1, :] = jnp.sum(query_pair * block, axis=0, keepdims=True)
    key = unit(silu(rounded(project(wk[...]))), 1)
    query = unit(silu(rounded(project(wq[...]))), 1) * head_dim ** (-0.5)
    overlap = jnp.sum(query * key, axis=1, keepdims=True)
    overlap = lane_pair(overlap[:half], overlap[half:])
    value = packed(silu(rounded(project(wv[...]))))
    gate = packed(silu(rounded(project(wg[...]))))
    rates = project(w_rates[...])
    decay_in = lane_pair(rates[:half, 0:1], rates[half:, 0:1]) + shift[0]
    soft = jnp.maximum(decay_in, 0.0) + jnp.log1p(jnp.exp(-jnp.abs(decay_in)))
    keep = jnp.exp(-rate[0] * soft)
    beta = 1.0 / (1.0 + jnp.exp(-lane_pair(rates[:half, 1:2], rates[half:, 1:2])))
    corr = beta * (value - keep * from_key[...])
    reading = keep * from_query[...] + overlap * corr
    squared = reading * reading
    left = lax.broadcasted_iota(jnp.int32, squared.shape, 1) < head_dim
    means = [
        jnp.sum(jnp.where(side, squared, 0.0), axis=1, keepdims=True) / head_dim
        for side in (left, jnp.logical_not(left))
    ]
    reading_scale = lane_pair(lax.rsqrt(means[0] + EPS), lax.rsqrt(means[1] + EPS))
    gain_pair = jnp.concatenate([head_gain[...], head_gain[...]], axis=1)
    head_out = (reading * reading_scale * gain_pair * gate).astype(BF16)
    for tile in range(tiles):
        spread[tile] = head_out
    corr_out[...] = corr
    keep_out[...] = keep
    key_out[...] = key_across


def state_kernel(state, corr, keep, key_across, new_state):
    half = state.shape[0] // 2
    head_dim = key_across.shape[0]
    across = key_across[...]
    for t in range(half):
        u = half + t
        key_pair = lane_pair(across[:, t : t + 1], across[:, u : u + 1])
        block = jnp.concatenate([state[t], state[u]], axis=1)
        updated = keep[t : t + 1, :] * block + key_pair * corr[t : t + 1, :]
        new_state[t] = updated[:, :head_dim]
        new_state[u] = updated[:, head_dim:]


def mix_kernel(heads, w_mix, tokens, slots, residual, outgoing):
    tiles, half, width = heads.shape
    top, bottom = [], []
    for pair in range(tiles // 2):
        even, odd = heads[2 * pair].astype(F32), heads[2 * pair + 1].astype(F32)
        left = lax.broadcasted_iota(jnp.int32, even.shape, 1) < width // 2
        top.append(jnp.where(left, even, pltpu.roll(odd, width // 2, 1)))
        bottom.append(jnp.where(left, pltpu.roll(even, width // 2, 1), odd))
    rows = [jnp.concatenate(part, axis=1).astype(BF16) for part in (top, bottom)]
    mixed = jnp.dot(jnp.concatenate(rows, axis=0), w_mix[...], preferred_element_type=F32)
    own = (tokens[...].astype(F32) + mixed).astype(BF16)
    residual[...] = own
    first, second = slot_hits(slots, outgoing.shape[0])
    outgoing[...] = jnp.dot(first + second, own, preferred_element_type=F32).astype(BF16)


def spread_kernel(along_z, spread):
    planes = along_z.shape[0]
    cores, tiles, count, width = spread.shape
    capacity = count // planes
    rows = [along_z[plane].astype(F32) for plane in range(planes)]
    for core in range(cores):
        own = [row[core * capacity : (core + 1) * capacity] for row in rows]
        block = jnp.concatenate(own, axis=0).astype(BF16)
        for tile in range(tiles):
            spread[core, tile] = block


def expert_kernel(arrived, gain, w_gate, w_up, w_down, parts, normed):
    cores, tiles, count, width = arrived.shape
    for core in range(cores):
        squares = jnp.zeros((count, width), F32)
        for tile in range(tiles):
            x = arrived[core, tile].astype(F32)
            squares += x * x
        mean = jnp.sum(squares, axis=1, keepdims=True) / (tiles * width)
        scale = lax.rsqrt(mean + EPS)
        for tile in range(tiles):
            cols = slice(tile * width, (tile + 1) * width)
            x = arrived[core, tile].astype(F32) * scale * gain[:, cols]
            normed[core * count : (core + 1) * count, cols] = x.astype(BF16)
    rows = normed[...]
    gate = jnp.dot(rows, w_gate[...], preferred_element_type=F32)
    up = jnp.dot(rows, w_up[...], preferred_element_type=F32)
    hidden = (silu(gate) * up).astype(BF16)
    for pair in range(tiles // 2):
        cols = slice(2 * pair * width, 2 * (pair + 1) * width)
        part = jnp.dot(hidden, w_down[:, cols], preferred_element_type=F32).astype(BF16)
        for core in range(cores):
            own = part[core * count : (core + 1) * count]
            parts[core, 2 * pair] = own[:, :width]
            parts[core, 2 * pair + 1] = own[:, width:]


def total_kernel(planes, parts, back):
    cores, tiles, count, width = parts.shape
    capacity = count // planes
    sums = []
    for core in range(cores):
        total = parts[core, 0].astype(F32)
        for tile in range(1, tiles):
            total += parts[core, tile].astype(F32)
        sums.append(total)
    for plane in range(planes):
        own = [total[plane * capacity : (plane + 1) * capacity] for total in sums]
        back[plane] = jnp.concatenate(own, axis=0).astype(BF16)


def combine_kernel(returned, slots, weights, residual, layer_out):
    rows = returned[...]
    seqs = slots.shape[1]
    source = lax.broadcasted_iota(jnp.int32, (seqs, seqs), 0)
    target = lax.broadcasted_iota(jnp.int32, (seqs, seqs), 1)
    dims = (((0,), (0,)), ((), ()))
    weighted = residual[...].astype(F32)
    for choice, hit in enumerate(slot_hits(slots, rows.shape[0])):
        across = jnp.where(source == target, weights[choice : choice + 1, :], 0.0)
        weight = jnp.sum(across, axis=1, keepdims=True)
        weighted += lax.dot_general(hit, rows, dims, preferred_element_type=F32) * weight
    layer_out[...] = weighted.astype(BF16)


def shards(
    tokens,
    state,
    attn_gain,
    ffn_gain,
    w_query,
    w_key,
    w_value,
    w_output_gate,
    w_decay,
    w_beta,
    decay_rate,
    decay_shift,
    head_gain,
    w_mix_out,
    expert_ids,
    expert_weights,
    w_gate,
    w_up,
    w_down,
):
    planes = lax.axis_size("z")
    cores = lax.axis_size("c")
    tp_size = lax.axis_size(TP)
    seqs, width = tokens.shape
    head_dim = head_gain.shape[0]
    model_width = attn_gain.shape[0]
    top_count = expert_ids.shape[1]
    expert_total = planes * cores
    capacity = 2 * seqs * top_count // expert_total
    half = seqs // 2
    count = planes * capacity

    gathered = to_everyone(tokens, TP)

    slot_count = expert_total * capacity
    wide = (seqs, width)
    w_rates, slots = local_call(
        functools.partial(prepare_kernel, expert_total, capacity),
        [((8, model_width), BF16), ((top_count, seqs), jnp.int32)],
        [],
        1 << 35,
        expert_ids.T,
        w_decay.T,
        w_beta.T,
        scalars=(lax.axis_index(TP)[None],),
    )
    square = (half, 2 * head_dim)
    spread, corr, keep, key_across = local_call(
        attend_kernel,
        [((tp_size, *square), BF16), (square, F32), (square, F32), ((head_dim, seqs), F32)],
        [pltpu.VMEM((seqs, model_width), BF16), pltpu.VMEM(square, F32), pltpu.VMEM(square, F32)],
        1 << 30,
        gathered,
        attn_gain[None],
        w_query.T,
        w_key.T,
        w_value.T,
        w_output_gate.T,
        w_rates,
        head_gain[None],
        state[:, 0],
        scalars=(decay_rate, decay_shift),
    )
    heads = exchanged(spread, TP)
    (new_state,) = local_call(
        state_kernel, [((seqs, head_dim, head_dim), F32)], [], 1 << 30, state[:, 0], corr, keep, key_across
    )
    residual, outgoing = local_call(
        mix_kernel, [(wide, BF16), ((slot_count, width), BF16)], [], 1 << 28, heads, w_mix_out, tokens, slots
    )
    along_z = exchanged(outgoing.reshape(planes, cores * capacity, width), "z")
    (spread_rows,) = local_call(
        spread_kernel, [((cores, tp_size, count, width), BF16)], [], 1 << 28, along_z
    )
    arrived = exchanged(spread_rows.reshape(cores * tp_size, count, width), PLANE)
    (parts,) = local_call(
        expert_kernel,
        [((cores, tp_size, count, width), BF16)],
        [pltpu.VMEM((cores * count, model_width), BF16)],
        1 << 30,
        arrived.reshape(cores, tp_size, count, width),
        ffn_gain[None],
        w_gate[0],
        w_up[0],
        w_down[0],
    )
    parts = exchanged(parts.reshape(cores * tp_size, count, width), PLANE)
    (back,) = local_call(
        functools.partial(total_kernel, planes),
        [((planes, cores * capacity, width), BF16)],
        [],
        1 << 28,
        parts.reshape(cores, tp_size, count, width),
    )
    returned = exchanged(back, "z").reshape(expert_total * capacity, width)
    (layer_out,) = local_call(
        combine_kernel, [(wide, BF16)], [], 1 << 26, returned, slots, expert_weights.T, residual
    )
    return (layer_out, new_state[:, None])


def solution(mesh):
    axes = Mesh(mesh.devices.reshape(16, 2, 4, 4), ("z", "c", "y", "x"))
    ep = ("z", "c")
    in_specs = (
        P(ep, TP),
        P(ep, TP, None, None),
        P(),
        P(),
        P(None, TP),
        P(None, TP),
        P(None, TP),
        P(None, TP),
        P(),
        P(),
        P(TP),
        P(TP),
        P(),
        P(None, TP),
        P(ep, None),
        P(ep, None),
        P(ep, None, TP),
        P(ep, None, TP),
        P(ep, TP, None),
    )
    out_specs = (P(ep, TP), P(ep, TP, None, None))
    return jax.shard_map(shards, mesh=axes, in_specs=in_specs, out_specs=out_specs, check_vma=False)
```

time: 148 us -> 120 us (0.81)
  blocking collectives: 50.7 us -> 81.2 us
  waiting for transfers between devices: 38.1 us -> 10.8 us
  matrix products: 17.3 us -> 0 us
  Pallas kernels: 0 us -> 10.3 us
  starting transfers between devices: 21 us -> 11.1 us
  local copies, waits for them, and re-layouts: 11 us -> 3.9 us
  other arithmetic: 6.99 us -> 0 us
    all_to_all x2 -> x4, blocking collectives: 50.7 us -> 81.2 us  [exchanged(): return lax.all_to_all(blocks, axes, 0, 0, tiled=True)]
    all_to_all x4 -> x2, waiting for transfers between devices: 38.1 us -> 10.8 us  [exchanged(): return lax.all_to_all(blocks, axes, 0, 0, tiled=True)]
    dot_general x15 -> x0, matrix products: 17.3 us -> none  [the longest x6 5.76 us: project(): return jnp.dot(normed, weight, preferred_element_type=jnp.float32)]
    pallas_call x0 -> x8, Pallas kernels: none -> 10.3 us  [local_call(): pl.pallas_call(kernel, out_shape=outs, in_specs=[vmem] * len(operands) +...]
    all_to_all x4 -> x2, starting transfers between devices: 21 us -> 11.1 us  [exchanged(): return lax.all_to_all(blocks, axes, 0, 0, tiled=True)]
    reshape x3 -> x0, local copies, waits for them, and re-layouts: 3.02 us -> none  [the longest x1 1.24 us: shards(): partial_value.reshape(cores, half_rows, tp_size, own_width)]
    reduce_sum x7 -> x0, other arithmetic: 2.85 us -> none  [the longest x1 1.37 us: shards(): summed = jnp.sum(parts, axis=1).astype(jnp.bfloat16)]
    unnamed x25 -> x34, local copies, waits for them, and re-layouts: 4.48 us -> 2.42 us
  transfers between devices with their start and end apart: 4 -> 2, of which waited for: 4 -> 2; matrix products, arithmetic and copies ran while one was open for 2% -> 0% of each run, Pallas kernels for 0% -> 4%
where the time goes in v2:
time: 120 us
  blocking collectives  81.2 us (68%)
  starting transfers between devices  11.1 us (9%)
  waiting for transfers between devices  10.8 us (9%)
  Pallas kernels  10.3 us (9%)
  local copies, waits for them, and re-layouts  3.9 us (3%)
  between operations  2.27 us (2%)
    all_to_all x4, blocking collectives, exchanged(): return lax.all_to_all(blocks, axes, 0, 0, tiled=True)  81.2 us
    all_to_all x2, starting transfers between devices, exchanged(): return lax.all_to_all(blocks, axes, 0, 0, tiled=True)  11.1 us
    all_to_all x2, waiting for transfers between devices, exchanged(): return lax.all_to_all(blocks, axes, 0, 0, tiled=True)  10.8 us
    pallas_call x8, Pallas kernels, local_call(): pl.pallas_call(kernel, out_shape=outs, in_specs=[vmem] * len(operands) +...  10.3 us
    unnamed x34, local copies, waits for them, and re-layouts  2.42 us
  transfers between devices with their start and end apart: 2, of which 2 were waited for; matrix products, arithmetic and copies ran while one was open for 0% of the time, Pallas kernels for 4%

profile of v2, /device:TPU:1, one launch (start us, length us, event | category | flops | bytes accessed | tf_op | source)
XLA Modules:
  0.0 119.6 jit_solution(10322887686443796374)
XLA Ops:
  0.6 1.5 %broadcast_in_dim.21 = bf16[16,64,128]{2,1,0:T(8,128)(2,1)} broadcast(bf16[64,128]{1,0:T(8,128)(2,1)} %tokens.1), dimensions={1,2} | broadcast | bytes 278528 | tf_op jit(solution)/shard_map/broadcast_in_dim | solution.py:24
  2.1 7.6 %all-to-all-start = ((bf16[16,64,128]{2,1,0:T(8,128)(2,1)}), bf16[16,64,128]{2,1,0:T(8,128)(2,1)S(1)}, u32[]{:S(2)}, u32[]{:S(2)}) async-start(bf16[16,64,128]{2,1,0:T(8,128)(2,1)} %broadcast_in_dim.21), calls=%async_computation | async-start | bytes 524288 | tf_op jit(solution)/shard_map/all_to_all | solution.py:19
  9.7 0.0 copy-start.11
  9.7 0.8 copy-done.11
  10.5 0.8 copy-done.12
  11.4 0.7 copy-done.14
  12.1 0.0 copy-start.9
  12.1 0.0 copy-start.13
  12.1 0.0 copy-start.16
  12.1 0.2 shard_map.194
  13.7 3.6 %all-to-all-done.tok = bf16[16,64,128]{2,1,0:T(8,128)(2,1)S(1)} async-done(((bf16[16,64,128]{2,1,0:T(8,128)(2,1)}), bf16[16,64,128]{2,1,0:T(8,128)(2,1)S(1)}, u32[]{:S(2)}, u32[]{:S(2)}) %all-to-all-start) | async-done | bytes 262176 | tf_op jit(solution)/shard_map/all_to_all | solution.py:19
  17.4 0.0 copy-done
  17.4 0.0 copy-done.7
  17.4 0.0 copy-start.4
  17.4 0.0 copy-start.10
  17.5 2.2 %shard_map.195 = (bf16[16,32,128]{2,1,0:T(8,128)(2,1)S(1)}, f32[32,128]{1,0:T(8,128)S(1)}, f32[32,128]{1,0:T(8,128)S(1)}, f32[64,64]{1,0:T(8,128)S(1)}) custom-call(bf16[16,64,128]{2,1,0:T(8,128)(2,1)S(1)} %all-to-all-done.tok, f32[1,2048]{1,0:T(1,128)S(1)} %bitcast.43, bf16[64,2048]{1,0:T(8,128)(2,1)S(1)} %bitcast.37, bf16[64,2048]{1,0:T(8,128)(2,1)S(1)} %bitcast.38, ...), custom_call_target="tpu_custom_call" | custom-call | flops 1073741824 | bytes 1048576 | tf_op jit(solution)/shard_map/pallas_call | solution.py:39
  19.7 9.7 %all_to_all.30.heads = bf16[16,32,128]{2,1,0:T(8,128)(2,1)S(1)} all-to-all(bf16[16,32,128]{2,1,0:T(8,128)(2,1)S(1)} %get-tuple-element.11), channel_id=1, replica_groups=mesh['z'=16,'c'=2,'y'=4,'x'=4] {'y','x'}, dimensions={0} | all-to-all | bytes 262144 | tf_op jit(solution)/shard_map/all_to_all | solution.py:19
  29.4 0.0 copy-done.4
  29.4 0.0 copy-start.3
  29.4 0.0 copy-start.5
  29.4 0.4 shard_map.196
  29.8 26.4 %all_to_all.31.along_z = bf16[16,16,128]{2,1,0:T(8,128)(2,1)S(1)} all-to-all(bf16[16,16,128]{2,1,0:T(8,128)(2,1)S(1)} %bitcast.35), channel_id=1, replica_groups=mesh['z'=16,'c'=2,'y'=4,'x'=4] {'z'}, dimensions={0} | all-to-all | bytes 131072 | tf_op jit(solution)/shard_map/all_to_all | solution.py:19
  56.3 0.2 shard_map.197
  56.5 24.3 %all_to_all.32 = bf16[32,128,128]{2,1,0:T(8,128)(2,1)S(1)} all-to-all(bf16[32,128,128]{2,1,0:T(8,128)(2,1)S(1)} %bitcast.27), channel_id=1, replica_groups=mesh['z'=16,'c'=2,'y'=4,'x'=4] {'c','y','x'}, dimensions={0} | all-to-all | bytes 2097152 | tf_op jit(solution)/shard_map/all_to_all | solution.py:19
  80.8 1.3 %shard_map.198 = bf16[2,16,128,128]{3,2,1,0:T(8,128)(2,1)S(1)} custom-call(bf16[2,16,128,128]{3,2,1,0:T(8,128)(2,1)S(1)} %bitcast.25, f32[1,2048]{1,0:T(1,128)S(1)} %bitcast.36, bf16[2048,256]{1,0:T(8,128)(2,1)S(1)} %bitcast.31, bf16[2048,256]{1,0:T(8,128)(2,1)S(1)} %bitcast.32, bf16[256,2048]{1,0:T(8,128)(2,1)S(1)} %bitcast.33), custom_call_target="tpu_custom_call" | custom-call | flops 1073741824 | bytes 1048576 | tf_op jit(solution)/shard_map/pallas_call | solution.py:39
  82.1 20.8 %all_to_all.33 = bf16[32,128,128]{2,1,0:T(8,128)(2,1)S(1)} all-to-all(bf16[32,128,128]{2,1,0:T(8,128)(2,1)S(1)} %bitcast.26), channel_id=1, replica_groups=mesh['z'=16,'c'=2,'y'=4,'x'=4] {'c','y','x'}, dimensions={0} | all-to-all | bytes 2097152 | tf_op jit(solution)/shard_map/all_to_all | solution.py:19
  102.8 0.8 shard_map.199
  103.6 3.5 %all-to-all-start.5 = ((bf16[16,16,128]{2,1,0:T(8,128)(2,1)}), bf16[16,16,128]{2,1,0:T(8,128)(2,1)S(1)}, u32[]{:S(2)}, u32[]{:S(2)}) async-start(bf16[16,16,128]{2,1,0:T(8,128)(2,1)} %shard_map.199), calls=%async_computation.5 | async-start | bytes 131072 | tf_op jit(solution)/shard_map/all_to_all | solution.py:19
  107.1 0.0 copy-start.15
  107.1 4.4 %shard_map.201 = f32[64,64,64]{2,1,0:T(8,128)} custom-call(f32[64,64,64]{2,1,0:T(8,128)S(1)} %bitcast.30, f32[32,128]{1,0:T(8,128)S(1)} %get-tuple-element.15.corr, f32[32,128]{1,0:T(8,128)S(1)} %get-tuple-element.16.keep, f32[64,64]{1,0:T(8,128)S(1)} %get-tuple-element.17.key_across), custom_call_target="tpu_custom_call" | custom-call | flops 1073741824 | bytes 1048576 | tf_op jit(solution)/shard_map/pallas_call | solution.py:39
  111.5 7.2 %all-to-all-done.5 = bf16[16,16,128]{2,1,0:T(8,128)(2,1)S(1)} async-done(((bf16[16,16,128]{2,1,0:T(8,128)(2,1)}), bf16[16,16,128]{2,1,0:T(8,128)(2,1)S(1)}, u32[]{:S(2)}, u32[]{:S(2)}) %all-to-all-start.5) | async-done | bytes 65568 | tf_op jit(solution)/shard_map/all_to_all | solution.py:19
  118.7 0.8 shard_map.200
  (19 shorter events, 0.0 us)
Async XLA Ops:
  2.1 15.3 %all-to-all-start = ((bf16[16,64,128]{2,1,0:T(8,128)(2,1)}), bf16[16,64,128]{2,1,0:T(8,128)(2,1)S(1)}, u32[]{:S(2)}, u32[]{:S(2)}) async-start(bf16[16,64,128]{2,1,0:T(8,128)(2,1)} %broadcast_in_dim.21), calls=%async_computation | async-start | bytes 524288 | tf_op jit(solution)/shard_map/all_to_all | solution.py:19
  9.7 0.8 copy-start.11
  10.5 0.8 copy-start.12
  11.4 0.7 copy-start.14
  12.1 5.3 %copy-start = (f32[64,1,64,64]{3,2,1,0:T(8,128)S(1)}, f32[64,1,64,64]{3,2,1,0:T(8,128)}, u32[]{:S(2)}) copy-start(f32[64,1,64,64]{3,2,1,0:T(8,128)} %param.20) | copy-start | bytes 3145732
  12.1 5.3 %copy-start.6 = (bf16[2048,64]{0,1:T(8,128)(2,1)S(1)}, bf16[2048,64]{0,1:T(8,128)(2,1)}, u32[]{:S(2)}) copy-start(bf16[2048,64]{0,1:T(8,128)(2,1)} %param.23) | copy-start | bytes 786436
  12.1 5.3 %copy-start.7 = (bf16[2048,64]{0,1:T(8,128)(2,1)S(1)}, bf16[2048,64]{0,1:T(8,128)(2,1)}, u32[]{:S(2)}) copy-start(bf16[2048,64]{0,1:T(8,128)(2,1)} %param.24) | copy-start | bytes 786436
  12.1 5.3 %copy-start.8 = (bf16[2048,64]{0,1:T(8,128)(2,1)S(1)}, bf16[2048,64]{0,1:T(8,128)(2,1)}, u32[]{:S(2)}) copy-start(bf16[2048,64]{0,1:T(8,128)(2,1)} %param.25) | copy-start | bytes 786436
  12.1 5.3 %copy-start.9 = (bf16[2048,64]{0,1:T(8,128)(2,1)S(1)}, bf16[2048,64]{0,1:T(8,128)(2,1)}, u32[]{:S(2)}) copy-start(bf16[2048,64]{0,1:T(8,128)(2,1)} %param.26) | copy-start | bytes 786436
  12.1 5.3 %copy-start.13 = (f32[2048]{0:T(1024)S(1)}, f32[2048]{0:T(1024)}, u32[]{:S(2)}) copy-start(f32[2048]{0:T(1024)} %param.21) | copy-start | bytes 24580
  12.1 5.3 %copy-start.16 = (f32[64]{0:T(128)S(1)}, f32[64]{0:T(128)}, u32[]{:S(2)}) copy-start(f32[64]{0:T(128)} %param.31) | copy-start | bytes 772
  17.4 12.0 %copy-start.4 = (bf16[64,128]{1,0:T(8,128)(2,1)S(1)}, bf16[64,128]{1,0:T(8,128)(2,1)}, u32[]{:S(2)}) copy-start(bf16[64,128]{1,0:T(8,128)(2,1)} %tokens.1) | copy-start | bytes 49156
  17.4 12.0 %copy-start.10 = (bf16[1024,128]{1,0:T(8,128)(2,1)S(1)}, bf16[1024,128]{1,0:T(8,128)(2,1)}, u32[]{:S(2)}) copy-start(bf16[1024,128]{1,0:T(8,128)(2,1)} %w_mix.1) | copy-start | bytes 786436
  29.4 51.3 %copy-start.1 = (bf16[1,2048,256]{2,1,0:T(8,128)(2,1)S(1)}, bf16[1,2048,256]{2,1,0:T(8,128)(2,1)}, u32[]{:S(2)}) copy-start(bf16[1,2048,256]{2,1,0:T(8,128)(2,1)} %param.35) | copy-start | bytes 3145732
  29.4 51.3 %copy-start.2 = (bf16[1,2048,256]{2,1,0:T(8,128)(2,1)S(1)}, bf16[1,2048,256]{2,1,0:T(8,128)(2,1)}, u32[]{:S(2)}) copy-start(bf16[1,2048,256]{2,1,0:T(8,128)(2,1)} %param.36) | copy-start | bytes 3145732
  29.4 51.3 %copy-start.3 = (bf16[1,256,2048]{2,1,0:T(8,128)(2,1)S(1)}, bf16[1,256,2048]{2,1,0:T(8,128)(2,1)}, u32[]{:S(2)}) copy-start(bf16[1,256,2048]{2,1,0:T(8,128)(2,1)} %param.37) | copy-start | bytes 3145732
  29.4 51.3 %copy-start.5 = (f32[2048]{0:T(1024)S(1)}, f32[2048]{0:T(1024)}, u32[]{:S(2)}) copy-start(f32[2048]{0:T(1024)} %param.22) | copy-start | bytes 24580
  103.6 15.1 %all-to-all-start.5 = ((bf16[16,16,128]{2,1,0:T(8,128)(2,1)}), bf16[16,16,128]{2,1,0:T(8,128)(2,1)S(1)}, u32[]{:S(2)}, u32[]{:S(2)}) async-start(bf16[16,16,128]{2,1,0:T(8,128)(2,1)} %shard_map.199), calls=%async_computation.5 | async-start | bytes 131072 | tf_op jit(solution)/shard_map/all_to_all | solution.py:19
  107.1 11.6 %copy-start.15 = (f32[64,2]{0,1:T(2,128)S(1)}, f32[64,2]{0,1:T(2,128)}, u32[]{:S(2)}) copy-start(f32[64,2]{0,1:T(2,128)} %param.34) | copy-start | bytes 1540

commit v3 on v2

v3 whole, which is shorter than its diff:
```python
import functools

import jax
import jax.numpy as jnp
from jax import lax
from jax.experimental import pallas as pl
from jax.experimental.pallas import tpu as pltpu
from jax.sharding import Mesh, PartitionSpec as P

EPS = 1e-06
TP = ("y", "x")
PLANE = ("c", "y", "x")
BF16 = jnp.bfloat16
F32 = jnp.float32
VMEM_LIMIT = 12 << 20


def exchanged(blocks, axes):
    return lax.all_to_all(blocks, axes, 0, 0, tiled=True)


def silu(values):
    return values * (1.0 / (1.0 + jnp.exp(-values)))


def rounded(values):
    return values.astype(BF16).astype(F32)


def local_call(kernel, out_shapes, scratch, flops, *operands, far_outs=0):
    vmem = pl.BlockSpec(memory_space=pltpu.VMEM)
    outs = [jax.ShapeDtypeStruct(shape, dtype) for shape, dtype in out_shapes]
    return pl.pallas_call(
        kernel,
        out_shape=outs,
        in_specs=[vmem] * len(operands),
        out_specs=[vmem] * (len(outs) - far_outs) + [pl.BlockSpec(memory_space=pl.ANY)] * far_outs,
        scratch_shapes=scratch,
        compiler_params=pltpu.CompilerParams(vmem_limit_bytes=VMEM_LIMIT),
        cost_estimate=pl.CostEstimate(flops=flops, bytes_accessed=1 << 20, transcendentals=0),
    )(*operands)


def broadcast_kernel(shard, rate, shift, spread, rates):
    for tile in range(spread.shape[0]):
        spread[tile] = shard[...]
    row = lax.broadcasted_iota(jnp.int32, rates.shape, 0)
    rates[...] = jnp.where(row == 0, rate[...], shift[...])


def head_row(weight, head):
    values = weight[...].astype(F32)
    own = lax.broadcasted_iota(jnp.int32, values.shape, 0) == head
    return jnp.sum(jnp.where(own, values, 0.0), axis=0, keepdims=True)


def diagonal_masks(size):
    source = lax.broadcasted_iota(jnp.int32, (size, size), 0)
    target = lax.broadcasted_iota(jnp.int32, (size, size), 1)
    return source, target


def as_column(row):
    source, target = diagonal_masks(row.shape[1])
    return jnp.sum(jnp.where(source == target, row, 0.0), axis=1, keepdims=True)


def slot_rows(ids, expert_total, capacity):
    choices, seqs = ids.shape
    experts = lax.broadcasted_iota(jnp.int32, (expert_total, seqs), 0)
    chosen = [(ids[choice : choice + 1, :] == experts).astype(F32) for choice in range(choices)]
    source, target = diagonal_masks(seqs)
    before = (source < target).astype(F32).astype(BF16)
    earlier = jnp.dot((chosen[0] + chosen[1]).astype(BF16), before, preferred_element_type=F32)
    slots = []
    for choice in range(choices):
        rank = jnp.sum(earlier * chosen[choice], axis=0, keepdims=True).astype(jnp.int32)
        slots.append(ids[choice : choice + 1, :] * capacity + rank)
    return slots


def slot_hits(slots, slot_count):
    places = lax.broadcasted_iota(jnp.int32, (slot_count, slots[0].shape[1]), 0)
    return [(slot == places).astype(F32).astype(BF16) for slot in slots]


def lane_pair(left, right):
    shape = (left.shape[0], 128)
    lane = lax.broadcasted_iota(jnp.int32, shape, 1)
    return jnp.where(lane < 64, jnp.broadcast_to(left, shape), jnp.broadcast_to(right, shape))


def attend_kernel(tok, gain, wq, wk, wv, wg, w_decay, w_beta, head_gain, rates_in, state,
                  spread, new_state, normed, blocks, keys, from_key, from_query):
    tiles, seqs, width = tok.shape
    head_dim = wq.shape[0]
    half = seqs // 2
    squares = jnp.zeros((seqs, width), F32)
    for tile in range(tiles):
        x = tok[tile].astype(F32)
        squares += x * x
    mean = jnp.sum(squares, axis=1, keepdims=True) / (tiles * width)
    scale = lax.rsqrt(mean + EPS)
    for tile in range(tiles):
        cols = slice(tile * width, (tile + 1) * width)
        normed[:, cols] = (tok[tile].astype(F32) * scale * gain[:, cols]).astype(BF16)
    rows = normed[...]
    dims = (((1,), (1,)), ((), ()))

    def unit(values):
        return values * lax.rsqrt(jnp.sum(values * values, axis=0, keepdims=True) + EPS)

    across = lax.dot_general(
        jnp.concatenate([wq[...], wk[...]], axis=0), rows, dims, preferred_element_type=F32
    )
    across = silu(rounded(across))
    query = unit(across[:head_dim]) * head_dim ** (-0.5)
    key = unit(across[head_dim:])
    for t in range(half):
        u = half + t
        block = jnp.concatenate([state[t], state[u]], axis=1)
        key_pair = lane_pair(key[:, t : t + 1], key[:, u : u + 1])
        query_pair = lane_pair(query[:, t : t + 1], query[:, u : u + 1])
        blocks[t] = block
        keys[t] = key_pair
        from_key[t : t + 1, :] = jnp.sum(key_pair * block, axis=0, keepdims=True)
        from_query[t : t + 1, :] = jnp.sum(query_pair * block, axis=0, keepdims=True)
    overlap = as_column(jnp.sum(query * key, axis=0, keepdims=True))
    overlap = lane_pair(overlap[:half], overlap[half:])
    own = lax.dot_general(rows, jnp.concatenate([wv[...], wg[...]], axis=0), dims, preferred_element_type=F32)
    own = silu(rounded(own))
    upper, lower = own[:half], own[half:]
    left = lax.broadcasted_iota(jnp.int32, upper.shape, 1) < head_dim
    value = jnp.where(left, upper, pltpu.roll(lower, head_dim, 1))
    gate = jnp.where(left, pltpu.roll(upper, head_dim, 1), lower)
    head = lax.axis_index("y") * lax.axis_size("x") + lax.axis_index("x")
    place = lax.broadcasted_iota(jnp.int32, (8, tiles * width), 0)
    w_rates = jnp.where(place == 0, head_row(w_decay, head), jnp.where(place == 1, head_row(w_beta, head), 0.0))
    rates = lax.dot_general(rows, w_rates.astype(BF16), dims, preferred_element_type=F32)
    decay_in = lane_pair(rates[:half, 0:1], rates[half:, 0:1]) + rates_in[1:2, :]
    soft = jnp.maximum(decay_in, 0.0) + jnp.log1p(jnp.exp(-jnp.abs(decay_in)))
    keep = jnp.exp(-rates_in[0:1, :] * soft)
    beta = 1.0 / (1.0 + jnp.exp(-lane_pair(rates[:half, 1:2], rates[half:, 1:2])))
    corr = beta * (value - keep * from_key[...])
    reading = keep * from_query[...] + overlap * corr
    squared = reading * reading
    means = [
        jnp.sum(jnp.where(side, squared, 0.0), axis=1, keepdims=True) / head_dim
        for side in (left, jnp.logical_not(left))
    ]
    reading_scale = lane_pair(lax.rsqrt(means[0] + EPS), lax.rsqrt(means[1] + EPS))
    gain_pair = jnp.concatenate([head_gain[...], head_gain[...]], axis=1)
    head_out = (reading * reading_scale * gain_pair * gate).astype(BF16)
    for tile in range(tiles):
        spread[tile] = head_out
    for t in range(half):
        updated = keep[t : t + 1, :] * blocks[t] + keys[t] * corr[t : t + 1, :]
        new_state[t] = updated[:, :head_dim]
        new_state[half + t] = updated[:, head_dim:]


def mix_kernel(expert_total, heads, w_mix, tokens, ids, residual, outgoing, slots_out):
    tiles, half, width = heads.shape
    top, bottom = [], []
    for pair in range(tiles // 2):
        even, odd = heads[2 * pair].astype(F32), heads[2 * pair + 1].astype(F32)
        left = lax.broadcasted_iota(jnp.int32, even.shape, 1) < width // 2
        top.append(jnp.where(left, even, pltpu.roll(odd, width // 2, 1)))
        bottom.append(jnp.where(left, pltpu.roll(even, width // 2, 1), odd))
    rows = [jnp.concatenate(part, axis=1).astype(BF16) for part in (top, bottom)]
    mixed = jnp.dot(jnp.concatenate(rows, axis=0), w_mix[...], preferred_element_type=F32)
    own = (tokens[...].astype(F32) + mixed).astype(BF16)
    residual[...] = own
    slots = slot_rows(ids, expert_total, outgoing.shape[0] // expert_total)
    for choice, slot in enumerate(slots):
        slots_out[choice : choice + 1, :] = slot
    first, second = slot_hits(slots, outgoing.shape[0])
    outgoing[...] = jnp.dot(first + second, own, preferred_element_type=F32).astype(BF16)


def spread_kernel(along_z, spread):
    planes = along_z.shape[0]
    cores, tiles, count, width = spread.shape
    capacity = count // planes
    rows = [along_z[plane].astype(F32) for plane in range(planes)]
    for core in range(cores):
        own = [row[core * capacity : (core + 1) * capacity] for row in rows]
        block = jnp.concatenate(own, axis=0).astype(BF16)
        for tile in range(tiles):
            spread[core, tile] = block


def expert_kernel(arrived, gain, w_gate, w_up, w_down, state, parts, state_out, normed, sem):
    state_copy = pltpu.make_async_copy(state, state_out, sem)
    state_copy.start()
    cores, tiles, count, width = arrived.shape
    for core in range(cores):
        squares = jnp.zeros((count, width), F32)
        for tile in range(tiles):
            x = arrived[core, tile].astype(F32)
            squares += x * x
        mean = jnp.sum(squares, axis=1, keepdims=True) / (tiles * width)
        scale = lax.rsqrt(mean + EPS)
        for tile in range(tiles):
            cols = slice(tile * width, (tile + 1) * width)
            x = arrived[core, tile].astype(F32) * scale * gain[:, cols]
            normed[core * count : (core + 1) * count, cols] = x.astype(BF16)
    rows = normed[...]
    gate = jnp.dot(rows, w_gate[...], preferred_element_type=F32)
    up = jnp.dot(rows, w_up[...], preferred_element_type=F32)
    hidden = (silu(gate) * up).astype(BF16)
    for pair in range(tiles // 2):
        cols = slice(2 * pair * width, 2 * (pair + 1) * width)
        part = jnp.dot(hidden, w_down[:, cols], preferred_element_type=F32).astype(BF16)
        for core in range(cores):
            own = part[core * count : (core + 1) * count]
            parts[core, 2 * pair] = own[:, :width]
            parts[core, 2 * pair + 1] = own[:, width:]
    state_copy.wait()


def total_kernel(planes, parts, back):
    cores, tiles, count, width = parts.shape
    capacity = count // planes
    sums = []
    for core in range(cores):
        total = parts[core, 0].astype(F32)
        for tile in range(1, tiles):
            total += parts[core, tile].astype(F32)
        sums.append(total)
    for plane in range(planes):
        own = [total[plane * capacity : (plane + 1) * capacity] for total in sums]
        back[plane] = jnp.concatenate(own, axis=0).astype(BF16)


def combine_kernel(returned, slots, weights, residual, layer_out):
    rows = returned[...]
    dims = (((0,), (0,)), ((), ()))
    weighted = residual[...].astype(F32)
    owners = [slots[choice : choice + 1, :] for choice in range(slots.shape[0])]
    for choice, hit in enumerate(slot_hits(owners, rows.shape[0])):
        pair = lax.dot_general(hit, rows, dims, preferred_element_type=F32)
        weighted += pair * as_column(weights[choice : choice + 1, :])
    layer_out[...] = weighted.astype(BF16)


def shards(
    tokens,
    state,
    attn_gain,
    ffn_gain,
    w_query,
    w_key,
    w_value,
    w_output_gate,
    w_decay,
    w_beta,
    decay_rate,
    decay_shift,
    head_gain,
    w_mix_out,
    expert_ids,
    expert_weights,
    w_gate,
    w_up,
    w_down,
):
    planes = lax.axis_size("z")
    cores = lax.axis_size("c")
    tp_size = lax.axis_size(TP)
    seqs, width = tokens.shape
    head_dim = head_gain.shape[0]
    model_width = attn_gain.shape[0]
    top_count = expert_ids.shape[1]
    expert_total = planes * cores
    capacity = 2 * seqs * top_count // expert_total
    half = seqs // 2
    count = planes * capacity

    slot_count = expert_total * capacity
    wide = (seqs, width)
    token_spread, head_rates = local_call(
        broadcast_kernel,
        [((tp_size, *wide), BF16), ((2, 2 * head_dim), F32)],
        [],
        1 << 35,
        tokens,
        decay_rate[None],
        decay_shift[None],
    )
    gathered = exchanged(token_spread, TP)
    square = (half, 2 * head_dim)
    blocks = (half, head_dim, 2 * head_dim)
    spread, new_state = local_call(
        attend_kernel,
        [((tp_size, *square), BF16), ((seqs, head_dim, head_dim), F32)],
        [
            pltpu.VMEM((seqs, model_width), BF16),
            pltpu.VMEM(blocks, F32),
            pltpu.VMEM(blocks, F32),
            pltpu.VMEM(square, F32),
            pltpu.VMEM(square, F32),
        ],
        1 << 30,
        gathered,
        attn_gain[None],
        w_query.T,
        w_key.T,
        w_value.T,
        w_output_gate.T,
        w_decay.T,
        w_beta.T,
        head_gain[None],
        head_rates,
        state[:, 0],
    )
    heads = exchanged(spread, TP)
    residual, outgoing, slots = local_call(
        functools.partial(mix_kernel, expert_total),
        [(wide, BF16), ((slot_count, width), BF16), ((top_count, seqs), jnp.int32)],
        [],
        1 << 28,
        heads,
        w_mix_out,
        tokens,
        expert_ids.T,
    )
    along_z = exchanged(outgoing.reshape(planes, cores * capacity, width), "z")
    (spread_rows,) = local_call(
        spread_kernel, [((cores, tp_size, count, width), BF16)], [], 1 << 28, along_z
    )
    arrived = exchanged(spread_rows.reshape(cores * tp_size, count, width), PLANE)
    parts, state_out = local_call(
        expert_kernel,
        [((cores, tp_size, count, width), BF16), (new_state.shape, F32)],
        [pltpu.VMEM((cores * count, model_width), BF16), pltpu.SemaphoreType.DMA],
        1 << 30,
        arrived.reshape(cores, tp_size, count, width),
        ffn_gain[None],
        w_gate[0],
        w_up[0],
        w_down[0],
        new_state,
        far_outs=1,
    )
    parts = exchanged(parts.reshape(cores * tp_size, count, width), PLANE)
    (back,) = local_call(
        functools.partial(total_kernel, planes),
        [((planes, cores * capacity, width), BF16)],
        [],
        1 << 28,
        parts.reshape(cores, tp_size, count, width),
    )
    returned = exchanged(back, "z").reshape(expert_total * capacity, width)
    (layer_out,) = local_call(
        combine_kernel, [(wide, BF16)], [], 1 << 26, returned, slots, expert_weights.T, residual
    )
    return (layer_out, state_out[:, None])


def solution(mesh):
    axes = Mesh(mesh.devices.reshape(16, 2, 4, 4), ("z", "c", "y", "x"))
    ep = ("z", "c")
    in_specs = (
        P(ep, TP),
        P(ep, TP, None, None),
        P(),
        P(),
        P(None, TP),
        P(None, TP),
        P(None, TP),
        P(None, TP),
        P(),
        P(),
        P(TP),
        P(TP),
        P(),
        P(None, TP),
        P(ep, None),
        P(ep, None),
        P(ep, None, TP),
        P(ep, None, TP),
        P(ep, TP, None),
    )
    out_specs = (P(ep, TP), P(ep, TP, None, None))
    return jax.shard_map(shards, mesh=axes, in_specs=in_specs, out_specs=out_specs, check_vma=False)
```

time: 120 us -> 120 us (level)
  blocking collectives: 81.2 us -> 111 us
  starting transfers between devices: 11.1 us -> 0 us
  waiting for transfers between devices: 10.8 us -> 0 us
  Pallas kernels: 10.3 us -> 5.59 us
  local copies, waits for them, and re-layouts: 3.9 us -> 0.8 us
    all_to_all x4 -> x6, blocking collectives: 81.2 us -> 111 us  [exchanged(): return lax.all_to_all(blocks, axes, 0, 0, tiled=True)]
    all_to_all x2 -> x0, starting transfers between devices: 11.1 us -> none  [exchanged(): return lax.all_to_all(blocks, axes, 0, 0, tiled=True)]
    all_to_all x2 -> x0, waiting for transfers between devices: 10.8 us -> none  [exchanged(): return lax.all_to_all(blocks, axes, 0, 0, tiled=True)]
    pallas_call x8 -> x7, Pallas kernels: 10.3 us -> 5.59 us  [local_call(): pl.pallas_call(kernel, out_shape=outs, in_specs=[vmem] * len(operands), o...]
    unnamed x34 -> x36, local copies, waits for them, and re-layouts: 2.42 us -> 0.8 us
    broadcast_in_dim x1 -> x0, local copies, waits for them, and re-layouts: 1.47 us -> none  [to_everyone(): return exchanged(jnp.broadcast_to(shard[None], (count, *shard.shape)), axes)]
  transfers between devices with their start and end apart: 2 -> 0, of which waited for: 2 -> 0; matrix products, arithmetic and copies ran while one was open for 0% -> 0% of each run, Pallas kernels for 4% -> 0%
where the time goes in v3:
time: 120 us; the launch traced here: 119 us
  blocking collectives  111 us (92%)
  Pallas kernels  5.59 us (5%)
  between operations  2.14 us (2%)
    all_to_all x6, blocking collectives, exchanged(): return lax.all_to_all(blocks, axes, 0, 0, tiled=True)  111 us
    pallas_call x7, Pallas kernels, local_call(): pl.pallas_call(kernel, out_shape=outs, in_specs=[vmem] * len(operands), o...  5.59 us

profile of v3, /device:TPU:1, one launch (start us, length us, event | category | flops | bytes accessed | tf_op | source)
XLA Modules:
  0.0 119.5 jit_solution(5515244300732933904)
XLA Ops:
  1.9 0.0 copy-start.12
  1.9 0.7 copy-done.12
  2.7 0.0 copy-start.8
  2.7 0.0 copy-start.10
  2.7 0.0 copy-start.11
  2.7 0.0 copy-start.14
  2.7 0.0 copy-start.17
  2.7 0.1 shard_map.194
  2.8 15.2 %all_to_all.30.tok = bf16[16,64,128]{2,1,0:T(8,128)(2,1)S(1)} all-to-all(bf16[16,64,128]{2,1,0:T(8,128)(2,1)S(1)} %get-tuple-element.11), channel_id=1, replica_groups=mesh['z'=16,'c'=2,'y'=4,'x'=4] {'y','x'}, dimensions={0} | all-to-all | bytes 524288 | tf_op jit(solution)/shard_map/all_to_all | solution.py:19
  18.0 0.0 copy-done.4
  18.0 0.0 copy-done.5
  18.0 0.0 copy-done.6
  18.0 0.0 copy-start.9
  18.0 0.0 copy-start.13
  18.0 0.0 copy-start.15
  18.1 2.6 %shard_map.195 = (bf16[16,32,128]{2,1,0:T(8,128)(2,1)S(1)}, f32[64,64,64]{2,1,0:T(8,128)S(1)}) custom-call(bf16[16,64,128]{2,1,0:T(8,128)(2,1)S(1)} %all_to_all.30.tok, f32[1,2048]{1,0:T(1,128)S(1)} %bitcast.45, bf16[64,2048]{1,0:T(8,128)(2,1)S(1)} %bitcast.39, bf16[64,2048]{1,0:T(8,128)(2,1)S(1)} %bitcast.40, bf16[64,2048]{1,0:T(8,128)(2,1)S(1)} %bitcast.41, ...), custom_call_target="tpu_custom_call" | custom-call | flops 1073741824 | bytes 1048576 | tf_op jit(solution)/shard_map/pallas_call | solution.py:33
  20.7 9.8 %all_to_all.31.heads = bf16[16,32,128]{2,1,0:T(8,128)(2,1)S(1)} all-to-all(bf16[16,32,128]{2,1,0:T(8,128)(2,1)S(1)} %get-tuple-element.13), channel_id=1, replica_groups=mesh['z'=16,'c'=2,'y'=4,'x'=4] {'y','x'}, dimensions={0} | all-to-all | bytes 262144 | tf_op jit(solution)/shard_map/all_to_all | solution.py:19
  30.4 0.0 copy-start
  30.4 0.0 copy-start.1
  30.5 0.0 copy-start.2
  30.5 0.0 copy-start.3
  30.5 0.4 shard_map.196
  30.9 26.4 %all_to_all.32.along_z = bf16[16,16,128]{2,1,0:T(8,128)(2,1)S(1)} all-to-all(bf16[16,16,128]{2,1,0:T(8,128)(2,1)S(1)} %bitcast.35), channel_id=1, replica_groups=mesh['z'=16,'c'=2,'y'=4,'x'=4] {'z'}, dimensions={0} | all-to-all | bytes 131072 | tf_op jit(solution)/shard_map/all_to_all | solution.py:19
  57.3 0.2 shard_map.197
  57.5 24.5 %all_to_all.33 = bf16[32,128,128]{2,1,0:T(8,128)(2,1)S(1)} all-to-all(bf16[32,128,128]{2,1,0:T(8,128)(2,1)S(1)} %bitcast.28), channel_id=1, replica_groups=mesh['z'=16,'c'=2,'y'=4,'x'=4] {'c','y','x'}, dimensions={0} | all-to-all | bytes 2097152 | tf_op jit(solution)/shard_map/all_to_all | solution.py:19
  82.0 0.0 copy-done.1
  82.0 1.3 %shard_map.198 = (bf16[2,16,128,128]{3,2,1,0:T(8,128)(2,1)S(1)}, f32[64,64,64]{2,1,0:T(8,128)}) custom-call(bf16[2,16,128,128]{3,2,1,0:T(8,128)(2,1)S(1)} %bitcast.30, f32[1,2048]{1,0:T(1,128)S(1)} %bitcast.37, bf16[2048,256]{1,0:T(8,128)(2,1)S(1)} %bitcast.32, bf16[2048,256]{1,0:T(8,128)(2,1)S(1)} %bitcast.33, bf16[256,2048]{1,0:T(8,128)(2,1)S(1)} %bitcast.34, ...), custom_call_target="tpu_custom_call" | custom-call | flops 1073741824 | bytes 1048576 | tf_op jit(solution)/shard_map/pallas_call | solution.py:33
  83.4 0.0 copy-start.16
  83.4 20.8 %all_to_all.34 = bf16[32,128,128]{2,1,0:T(8,128)(2,1)S(1)} all-to-all(bf16[32,128,128]{2,1,0:T(8,128)(2,1)S(1)} %bitcast.31), channel_id=1, replica_groups=mesh['z'=16,'c'=2,'y'=4,'x'=4] {'c','y','x'}, dimensions={0} | all-to-all | bytes 2097152 | tf_op jit(solution)/shard_map/all_to_all | solution.py:19
  104.2 0.1 shard_map.199
  104.3 14.3 %all_to_all.35 = bf16[16,16,128]{2,1,0:T(8,128)(2,1)S(1)} all-to-all(bf16[16,16,128]{2,1,0:T(8,128)(2,1)S(1)} %shard_map.199), channel_id=1, replica_groups=mesh['z'=16,'c'=2,'y'=4,'x'=4] {'z'}, dimensions={0} | all-to-all | bytes 131072 | tf_op jit(solution)/shard_map/all_to_all | solution.py:19
  118.6 0.8 shard_map.200
  (17 shorter events, 0.0 us)
Async XLA Ops:
  1.9 0.7 copy-start.12
  2.6 15.3 %copy-start.4 = (f32[64,1,64,64]{3,2,1,0:T(8,128)S(1)}, f32[64,1,64,64]{3,2,1,0:T(8,128)}, u32[]{:S(2)}) copy-start(f32[64,1,64,64]{3,2,1,0:T(8,128)} %param.20) | copy-start | bytes 3145732
  2.6 15.3 %copy-start.5 = (bf16[2048,64]{0,1:T(8,128)(2,1)S(1)}, bf16[2048,64]{0,1:T(8,128)(2,1)}, u32[]{:S(2)}) copy-start(bf16[2048,64]{0,1:T(8,128)(2,1)} %param.23) | copy-start | bytes 786436
  2.6 15.3 %copy-start.6 = (bf16[2048,64]{0,1:T(8,128)(2,1)S(1)}, bf16[2048,64]{0,1:T(8,128)(2,1)}, u32[]{:S(2)}) copy-start(bf16[2048,64]{0,1:T(8,128)(2,1)} %param.24) | copy-start | bytes 786436
  2.7 15.3 %copy-start.7 = (bf16[2048,64]{0,1:T(8,128)(2,1)S(1)}, bf16[2048,64]{0,1:T(8,128)(2,1)}, u32[]{:S(2)}) copy-start(bf16[2048,64]{0,1:T(8,128)(2,1)} %param.25) | copy-start | bytes 786436
  2.7 15.3 %copy-start.8 = (bf16[2048,64]{0,1:T(8,128)(2,1)S(1)}, bf16[2048,64]{0,1:T(8,128)(2,1)}, u32[]{:S(2)}) copy-start(bf16[2048,64]{0,1:T(8,128)(2,1)} %param.26) | copy-start | bytes 786436
  2.7 15.3 %copy-start.10 = (bf16[2048,16]{0,1:T(8,128)(2,1)S(1)}, bf16[2048,16]{0,1:T(8,128)(2,1)}, u32[]{:S(2)}) copy-start(bf16[2048,16]{0,1:T(8,128)(2,1)} %param.27) | copy-start | bytes 196612
  2.7 15.3 %copy-start.11 = (bf16[2048,16]{0,1:T(8,128)(2,1)S(1)}, bf16[2048,16]{0,1:T(8,128)(2,1)}, u32[]{:S(2)}) copy-start(bf16[2048,16]{0,1:T(8,128)(2,1)} %param.28) | copy-start | bytes 196612
  2.7 15.3 %copy-start.14 = (f32[2048]{0:T(1024)S(1)}, f32[2048]{0:T(1024)}, u32[]{:S(2)}) copy-start(f32[2048]{0:T(1024)} %param.21) | copy-start | bytes 24580
  2.7 15.3 %copy-start.17 = (f32[64]{0:T(128)S(1)}, f32[64]{0:T(128)}, u32[]{:S(2)}) copy-start(f32[64]{0:T(128)} %param.31) | copy-start | bytes 772
  18.0 12.4 %copy-start.9 = (bf16[1024,128]{1,0:T(8,128)(2,1)S(1)}, bf16[1024,128]{1,0:T(8,128)(2,1)}, u32[]{:S(2)}) copy-start(bf16[1024,128]{1,0:T(8,128)(2,1)} %w_mix.1) | copy-start | bytes 786436
  18.0 12.4 %copy-start.13 = (bf16[64,128]{1,0:T(8,128)(2,1)S(1)}, bf16[64,128]{1,0:T(8,128)(2,1)}, u32[]{:S(2)}) copy-start(bf16[64,128]{1,0:T(8,128)(2,1)} %tokens.1) | copy-start | bytes 49156
  18.0 12.4 %copy-start.15 = (s32[64,2]{0,1:T(2,128)S(1)}, s32[64,2]{0,1:T(2,128)}, u32[]{:S(2)}) copy-start(s32[64,2]{0,1:T(2,128)} %param.33) | copy-start | bytes 1540
  30.4 51.6 %copy-start = (bf16[1,2048,256]{2,1,0:T(8,128)(2,1)S(1)}, bf16[1,2048,256]{2,1,0:T(8,128)(2,1)}, u32[]{:S(2)}) copy-start(bf16[1,2048,256]{2,1,0:T(8,128)(2,1)} %param.35) | copy-start | bytes 3145732
  30.4 51.6 %copy-start.1 = (bf16[1,2048,256]{2,1,0:T(8,128)(2,1)S(1)}, bf16[1,2048,256]{2,1,0:T(8,128)(2,1)}, u32[]{:S(2)}) copy-start(bf16[1,2048,256]{2,1,0:T(8,128)(2,1)} %param.36) | copy-start | bytes 3145732
  30.5 51.6 %copy-start.2 = (bf16[1,256,2048]{2,1,0:T(8,128)(2,1)S(1)}, bf16[1,256,2048]{2,1,0:T(8,128)(2,1)}, u32[]{:S(2)}) copy-start(bf16[1,256,2048]{2,1,0:T(8,128)(2,1)} %param.37) | copy-start | bytes 3145732
  30.5 51.6 %copy-start.3 = (f32[2048]{0:T(1024)S(1)}, f32[2048]{0:T(1024)}, u32[]{:S(2)}) copy-start(f32[2048]{0:T(1024)} %param.22) | copy-start | bytes 24580
  83.4 35.3 %copy-start.16 = (f32[64,2]{0,1:T(2,128)S(1)}, f32[64,2]{0,1:T(2,128)}, u32[]{:S(2)}) copy-start(f32[64,2]{0,1:T(2,128)} %param.34) | copy-start | bytes 1540

commit v4 on v3

--- a/solution.py
+++ b/solution.py
@@ -95,6 +95,8 @@
     tiles, seqs, width = tok.shape
     head_dim = wq.shape[0]
     half = seqs // 2
+    for t in range(half):
+        blocks[t] = jnp.concatenate([state[t], state[half + t]], axis=1)
     squares = jnp.zeros((seqs, width), F32)
     for tile in range(tiles):
         x = tok[tile].astype(F32)
@@ -116,15 +118,23 @@
     across = silu(rounded(across))
     query = unit(across[:head_dim]) * head_dim ** (-0.5)
     key = unit(across[head_dim:])
-    for t in range(half):
-        u = half + t
-        block = jnp.concatenate([state[t], state[u]], axis=1)
-        key_pair = lane_pair(key[:, t : t + 1], key[:, u : u + 1])
-        query_pair = lane_pair(query[:, t : t + 1], query[:, u : u + 1])
-        blocks[t] = block
-        keys[t] = key_pair
-        from_key[t : t + 1, :] = jnp.sum(key_pair * block, axis=0, keepdims=True)
-        from_query[t : t + 1, :] = jnp.sum(query_pair * block, axis=0, keepdims=True)
+    both = jnp.concatenate([query, key], axis=0)
+    high = rounded(both)
+    terms = jnp.concatenate([high, both - high], axis=1).astype(BF16)
+    token = lax.broadcasted_iota(jnp.int32, (seqs, 4 * head_dim), 0)
+    lane = lax.broadcasted_iota(jnp.int32, (seqs, 4 * head_dim), 1)
+    owner = jnp.where(lane % (2 * head_dim) < head_dim, token, token - half) - lane // (2 * head_dim)
+    for t in range(0, half, 2):
+        chosen = (owner == t).astype(F32).astype(BF16)
+        repeated = jnp.dot(terms, jnp.concatenate([chosen, chosen], axis=0), preferred_element_type=F32)
+        for step in range(2):
+            row = t + step
+            block = blocks[row]
+            cols = slice(step * 2 * head_dim, (step + 1) * 2 * head_dim)
+            key_pair = repeated[head_dim:, cols]
+            keys[row] = key_pair
+            from_key[row : row + 1, :] = jnp.sum(key_pair * block, axis=0, keepdims=True)
+            from_query[row : row + 1, :] = jnp.sum(repeated[:head_dim, cols] * block, axis=0, keepdims=True)
     overlap = as_column(jnp.sum(query * key, axis=0, keepdims=True))
     overlap = lane_pair(overlap[:half], overlap[half:])
     own = lax.dot_general(rows, jnp.concatenate([wv[...], wg[...]], axis=0), dims, preferred_element_type=F32)

time: 120 us -> 119 us (level)
  no operation moved by 1% of the time
where the time goes in v4:
time: 119 us
  blocking collectives  111 us (93%)
  Pallas kernels  4.95 us (4%)
  between operations  2.15 us (2%)
    all_to_all x6, blocking collectives, exchanged(): return lax.all_to_all(blocks, axes, 0, 0, tiled=True)  111 us
    pallas_call x7, Pallas kernels, local_call(): pl.pallas_call(kernel, out_shape=outs, in_specs=[vmem] * len(operands), o...  4.95 us

profile of v4, /device:TPU:1, one launch (start us, length us, event | category | flops | bytes accessed | tf_op | source)
XLA Modules:
  0.0 118.8 jit_solution(256947659951225442)
XLA Ops:
  1.9 0.0 copy-start.12
  1.9 0.7 copy-done.12
  2.7 0.0 copy-start.8
  2.7 0.0 copy-start.10
  2.7 0.0 copy-start.11
  2.7 0.0 copy-start.14
  2.7 0.0 copy-start.17
  2.7 0.1 shard_map.194
  2.8 15.2 %all_to_all.30.tok = bf16[16,64,128]{2,1,0:T(8,128)(2,1)S(1)} all-to-all(bf16[16,64,128]{2,1,0:T(8,128)(2,1)S(1)} %get-tuple-element.11), channel_id=1, replica_groups=mesh['z'=16,'c'=2,'y'=4,'x'=4] {'y','x'}, dimensions={0} | all-to-all | bytes 524288 | tf_op jit(solution)/shard_map/all_to_all | solution.py:19
  18.0 0.0 copy-done.4
  18.0 0.0 copy-done.5
  18.0 0.0 copy-start.9
  18.0 0.0 copy-start.13
  18.0 0.0 copy-start.15
  18.1 2.0 %shard_map.195 = (bf16[16,32,128]{2,1,0:T(8,128)(2,1)S(1)}, f32[64,64,64]{2,1,0:T(8,128)S(1)}) custom-call(bf16[16,64,128]{2,1,0:T(8,128)(2,1)S(1)} %all_to_all.30.tok, f32[1,2048]{1,0:T(1,128)S(1)} %bitcast.45, bf16[64,2048]{1,0:T(8,128)(2,1)S(1)} %bitcast.39, bf16[64,2048]{1,0:T(8,128)(2,1)S(1)} %bitcast.40, bf16[64,2048]{1,0:T(8,128)(2,1)S(1)} %bitcast.41, ...), custom_call_target="tpu_custom_call" | custom-call | flops 1073741824 | bytes 1048576 | tf_op jit(solution)/shard_map/pallas_call | solution.py:33
  20.0 9.8 %all_to_all.31.heads = bf16[16,32,128]{2,1,0:T(8,128)(2,1)S(1)} all-to-all(bf16[16,32,128]{2,1,0:T(8,128)(2,1)S(1)} %get-tuple-element.13), channel_id=1, replica_groups=mesh['z'=16,'c'=2,'y'=4,'x'=4] {'y','x'}, dimensions={0} | all-to-all | bytes 262144 | tf_op jit(solution)/shard_map/all_to_all | solution.py:19
  29.8 0.0 copy-done.13
  29.8 0.0 copy-start
  29.8 0.0 copy-start.1
  29.8 0.0 copy-start.2
  29.8 0.0 copy-start.3
  29.9 0.4 shard_map.196
  30.3 26.4 %all_to_all.32.along_z = bf16[16,16,128]{2,1,0:T(8,128)(2,1)S(1)} all-to-all(bf16[16,16,128]{2,1,0:T(8,128)(2,1)S(1)} %bitcast.35), channel_id=1, replica_groups=mesh['z'=16,'c'=2,'y'=4,'x'=4] {'z'}, dimensions={0} | all-to-all | bytes 131072 | tf_op jit(solution)/shard_map/all_to_all | solution.py:19
  56.7 0.2 shard_map.197
  56.9 24.5 %all_to_all.33 = bf16[32,128,128]{2,1,0:T(8,128)(2,1)S(1)} all-to-all(bf16[32,128,128]{2,1,0:T(8,128)(2,1)S(1)} %bitcast.28), channel_id=1, replica_groups=mesh['z'=16,'c'=2,'y'=4,'x'=4] {'c','y','x'}, dimensions={0} | all-to-all | bytes 2097152 | tf_op jit(solution)/shard_map/all_to_all | solution.py:19
  81.4 1.3 %shard_map.198 = (bf16[2,16,128,128]{3,2,1,0:T(8,128)(2,1)S(1)}, f32[64,64,64]{2,1,0:T(8,128)}) custom-call(bf16[2,16,128,128]{3,2,1,0:T(8,128)(2,1)S(1)} %bitcast.30, f32[1,2048]{1,0:T(1,128)S(1)} %bitcast.37, bf16[2048,256]{1,0:T(8,128)(2,1)S(1)} %bitcast.32, bf16[2048,256]{1,0:T(8,128)(2,1)S(1)} %bitcast.33, bf16[256,2048]{1,0:T(8,128)(2,1)S(1)} %bitcast.34, ...), custom_call_target="tpu_custom_call" | custom-call | flops 1073741824 | bytes 1048576 | tf_op jit(solution)/shard_map/pallas_call | solution.py:33
  82.8 0.0 copy-start.16
  82.8 20.8 %all_to_all.34 = bf16[32,128,128]{2,1,0:T(8,128)(2,1)S(1)} all-to-all(bf16[32,128,128]{2,1,0:T(8,128)(2,1)S(1)} %bitcast.31), channel_id=1, replica_groups=mesh['z'=16,'c'=2,'y'=4,'x'=4] {'c','y','x'}, dimensions={0} | all-to-all | bytes 2097152 | tf_op jit(solution)/shard_map/all_to_all | solution.py:19
  103.5 0.1 shard_map.199
  103.7 14.3 %all_to_all.35 = bf16[16,16,128]{2,1,0:T(8,128)(2,1)S(1)} all-to-all(bf16[16,16,128]{2,1,0:T(8,128)(2,1)S(1)} %shard_map.199), channel_id=1, replica_groups=mesh['z'=16,'c'=2,'y'=4,'x'=4] {'z'}, dimensions={0} | all-to-all | bytes 131072 | tf_op jit(solution)/shard_map/all_to_all | solution.py:19
  118.0 0.0 copy-done.16
  118.0 0.8 shard_map.200
  (17 shorter events, 0.0 us)
Async XLA Ops:
  1.9 0.7 copy-start.12
  2.6 15.3 %copy-start.4 = (f32[64,1,64,64]{3,2,1,0:T(8,128)S(1)}, f32[64,1,64,64]{3,2,1,0:T(8,128)}, u32[]{:S(2)}) copy-start(f32[64,1,64,64]{3,2,1,0:T(8,128)} %param.20) | copy-start | bytes 3145732
  2.6 15.3 %copy-start.5 = (bf16[2048,64]{0,1:T(8,128)(2,1)S(1)}, bf16[2048,64]{0,1:T(8,128)(2,1)}, u32[]{:S(2)}) copy-start(bf16[2048,64]{0,1:T(8,128)(2,1)} %param.23) | copy-start | bytes 786436
  2.6 15.3 %copy-start.6 = (bf16[2048,64]{0,1:T(8,128)(2,1)S(1)}, bf16[2048,64]{0,1:T(8,128)(2,1)}, u32[]{:S(2)}) copy-start(bf16[2048,64]{0,1:T(8,128)(2,1)} %param.24) | copy-start | bytes 786436
  2.7 15.3 %copy-start.7 = (bf16[2048,64]{0,1:T(8,128)(2,1)S(1)}, bf16[2048,64]{0,1:T(8,128)(2,1)}, u32[]{:S(2)}) copy-start(bf16[2048,64]{0,1:T(8,128)(2,1)} %param.25) | copy-start | bytes 786436
  2.7 15.3 %copy-start.8 = (bf16[2048,64]{0,1:T(8,128)(2,1)S(1)}, bf16[2048,64]{0,1:T(8,128)(2,1)}, u32[]{:S(2)}) copy-start(bf16[2048,64]{0,1:T(8,128)(2,1)} %param.26) | copy-start | bytes 786436
  2.7 15.3 %copy-start.10 = (bf16[2048,16]{0,1:T(8,128)(2,1)S(1)}, bf16[2048,16]{0,1:T(8,128)(2,1)}, u32[]{:S(2)}) copy-start(bf16[2048,16]{0,1:T(8,128)(2,1)} %param.27) | copy-start | bytes 196612
  2.7 15.3 %copy-start.11 = (bf16[2048,16]{0,1:T(8,128)(2,1)S(1)}, bf16[2048,16]{0,1:T(8,128)(2,1)}, u32[]{:S(2)}) copy-start(bf16[2048,16]{0,1:T(8,128)(2,1)} %param.28) | copy-start | bytes 196612
  2.7 15.3 %copy-start.14 = (f32[2048]{0:T(1024)S(1)}, f32[2048]{0:T(1024)}, u32[]{:S(2)}) copy-start(f32[2048]{0:T(1024)} %param.21) | copy-start | bytes 24580
  2.7 15.3 %copy-start.17 = (f32[64]{0:T(128)S(1)}, f32[64]{0:T(128)}, u32[]{:S(2)}) copy-start(f32[64]{0:T(128)} %param.31) | copy-start | bytes 772
  18.0 11.8 %copy-start.9 = (bf16[1024,128]{1,0:T(8,128)(2,1)S(1)}, bf16[1024,128]{1,0:T(8,128)(2,1)}, u32[]{:S(2)}) copy-start(bf16[1024,128]{1,0:T(8,128)(2,1)} %w_mix.1) | copy-start | bytes 786436
  18.0 11.8 %copy-start.13 = (bf16[64,128]{1,0:T(8,128)(2,1)S(1)}, bf16[64,128]{1,0:T(8,128)(2,1)}, u32[]{:S(2)}) copy-start(bf16[64,128]{1,0:T(8,128)(2,1)} %tokens.1) | copy-start | bytes 49156
  18.0 11.8 %copy-start.15 = (s32[64,2]{0,1:T(2,128)S(1)}, s32[64,2]{0,1:T(2,128)}, u32[]{:S(2)}) copy-start(s32[64,2]{0,1:T(2,128)} %param.33) | copy-start | bytes 1540
  29.8 51.6 %copy-start = (bf16[1,2048,256]{2,1,0:T(8,128)(2,1)S(1)}, bf16[1,2048,256]{2,1,0:T(8,128)(2,1)}, u32[]{:S(2)}) copy-start(bf16[1,2048,256]{2,1,0:T(8,128)(2,1)} %param.35) | copy-start | bytes 3145732
  29.8 51.6 %copy-start.1 = (bf16[1,2048,256]{2,1,0:T(8,128)(2,1)S(1)}, bf16[1,2048,256]{2,1,0:T(8,128)(2,1)}, u32[]{:S(2)}) copy-start(bf16[1,2048,256]{2,1,0:T(8,128)(2,1)} %param.36) | copy-start | bytes 3145732
  29.8 51.6 %copy-start.2 = (bf16[1,256,2048]{2,1,0:T(8,128)(2,1)S(1)}, bf16[1,256,2048]{2,1,0:T(8,128)(2,1)}, u32[]{:S(2)}) copy-start(bf16[1,256,2048]{2,1,0:T(8,128)(2,1)} %param.37) | copy-start | bytes 3145732
  29.8 51.6 %copy-start.3 = (f32[2048]{0:T(1024)S(1)}, f32[2048]{0:T(1024)}, u32[]{:S(2)}) copy-start(f32[2048]{0:T(1024)} %param.22) | copy-start | bytes 24580
  82.8 35.3 %copy-start.16 = (f32[64,2]{0,1:T(2,128)S(1)}, f32[64,2]{0,1:T(2,128)}, u32[]{:S(2)}) copy-start(f32[64,2]{0,1:T(2,128)} %param.34) | copy-start | bytes 1540

commit v5 on v4

--- a/solution.py
+++ b/solution.py
@@ -41,7 +41,16 @@
     )(*operands)
 
 
-def broadcast_kernel(shard, rate, shift, spread, rates):
+def owner_kernel(owner):
+    seqs, columns = owner.shape
+    token = lax.broadcasted_iota(jnp.int32, owner.shape, 0)
+    lane = lax.broadcasted_iota(jnp.int32, owner.shape, 1)
+    row = columns // 2
+    owner[...] = jnp.where(lane % row < row // 2, token, token - seqs // 2) - lane // row
+
+
+def broadcast_kernel(shard, rate, shift, owner, spread, rates, owner_out):
+    owner_out[...] = owner[...]
     for tile in range(spread.shape[0]):
         spread[tile] = shard[...]
     row = lax.broadcasted_iota(jnp.int32, rates.shape, 0)
@@ -90,7 +99,7 @@
     return jnp.where(lane < 64, jnp.broadcast_to(left, shape), jnp.broadcast_to(right, shape))
 
 
-def attend_kernel(tok, gain, wq, wk, wv, wg, w_decay, w_beta, head_gain, rates_in, state,
+def attend_kernel(tok, gain, wq, wk, wv, wg, w_decay, w_beta, head_gain, rates_in, owner, state,
                   spread, new_state, normed, blocks, keys, from_key, from_query):
     tiles, seqs, width = tok.shape
     head_dim = wq.shape[0]
@@ -121,11 +130,8 @@
     both = jnp.concatenate([query, key], axis=0)
     high = rounded(both)
     terms = jnp.concatenate([high, both - high], axis=1).astype(BF16)
-    token = lax.broadcasted_iota(jnp.int32, (seqs, 4 * head_dim), 0)
-    lane = lax.broadcasted_iota(jnp.int32, (seqs, 4 * head_dim), 1)
-    owner = jnp.where(lane % (2 * head_dim) < head_dim, token, token - half) - lane // (2 * head_dim)
     for t in range(0, half, 2):
-        chosen = (owner == t).astype(F32).astype(BF16)
+        chosen = (owner[...] == t).astype(F32).astype(BF16)
         repeated = jnp.dot(terms, jnp.concatenate([chosen, chosen], axis=0), preferred_element_type=F32)
         for step in range(2):
             row = t + step
@@ -289,14 +295,16 @@
 
     slot_count = expert_total * capacity
     wide = (seqs, width)
-    token_spread, head_rates = local_call(
+    (owner,) = local_call(owner_kernel, [((seqs, 4 * head_dim), jnp.int32)], [], 1 << 35)
+    token_spread, head_rates, owner = local_call(
         broadcast_kernel,
-        [((tp_size, *wide), BF16), ((2, 2 * head_dim), F32)],
+        [((tp_size, *wide), BF16), ((2, 2 * head_dim), F32), (owner.shape, jnp.int32)],
         [],
         1 << 35,
         tokens,
         decay_rate[None],
         decay_shift[None],
+        owner,
     )
     gathered = exchanged(token_spread, TP)
     square = (half, 2 * head_dim)
@@ -322,6 +330,7 @@
         w_beta.T,
         head_gain[None],
         head_rates,
+        owner,
         state[:, 0],
     )
     heads = exchanged(spread, TP)

time: 119 us -> 119 us (level)
    pallas_call x7 -> x8, Pallas kernels: 4.95 us -> 4.97 us  [local_call(): pl.pallas_call(kernel, out_shape=outs, in_specs=[vmem] * len(operands), o...]
where the time goes in v5:
time: 119 us; the launch traced here: 118 us
  blocking collectives  111 us (93%)
  Pallas kernels  4.97 us (4%)
  between operations  2.16 us (2%)
    all_to_all x6, blocking collectives, exchanged(): return lax.all_to_all(blocks, axes, 0, 0, tiled=True)  111 us
    pallas_call x8, Pallas kernels, local_call(): pl.pallas_call(kernel, out_shape=outs, in_specs=[vmem] * len(operands), o...  4.97 us

profile of v5, /device:TPU:1, one launch (start us, length us, event | category | flops | bytes accessed | tf_op | source)
XLA Modules:
  0.0 118.2 jit_solution(2133397246729038068)
XLA Ops:
  0.6 0.0 copy-start.12
  2.0 0.0 copy-done.12
  2.0 0.0 copy-start.4
  2.0 0.0 copy-start.5
  2.0 0.0 copy-start.6
  2.0 0.0 copy-start.7
  2.0 0.0 copy-start.8
  2.0 0.0 copy-start.10
  2.0 0.0 copy-start.11
  2.0 0.0 copy-start.13
  2.1 0.0 copy-start.16
  2.1 0.1 shard_map.195
  2.1 15.2 %all_to_all.30.tok = bf16[16,64,128]{2,1,0:T(8,128)(2,1)S(1)} all-to-all(bf16[16,64,128]{2,1,0:T(8,128)(2,1)S(1)} %get-tuple-element.12), channel_id=1, replica_groups=mesh['z'=16,'c'=2,'y'=4,'x'=4] {'y','x'}, dimensions={0} | all-to-all | bytes 524288 | tf_op jit(solution)/shard_map/all_to_all | solution.py:19
  17.3 0.0 copy-done.5
  17.4 0.0 copy-start.9
  17.4 0.0 copy-start.14
  17.4 2.0 %shard_map.196 = (bf16[16,32,128]{2,1,0:T(8,128)(2,1)S(1)}, f32[64,64,64]{2,1,0:T(8,128)S(1)}) custom-call(bf16[16,64,128]{2,1,0:T(8,128)(2,1)S(1)} %all_to_all.30.tok, f32[1,2048]{1,0:T(1,128)S(1)} %bitcast.45, bf16[64,2048]{1,0:T(8,128)(2,1)S(1)} %bitcast.39, bf16[64,2048]{1,0:T(8,128)(2,1)S(1)} %bitcast.40, bf16[64,2048]{1,0:T(8,128)(2,1)S(1)} %bitcast.41, ...), custom_call_target="tpu_custom_call" | custom-call | flops 1073741824 | bytes 1048576 | tf_op jit(solution)/shard_map/pallas_call | solution.py:33
  19.4 9.7 %all_to_all.31.heads = bf16[16,32,128]{2,1,0:T(8,128)(2,1)S(1)} all-to-all(bf16[16,32,128]{2,1,0:T(8,128)(2,1)S(1)} %get-tuple-element.15), channel_id=1, replica_groups=mesh['z'=16,'c'=2,'y'=4,'x'=4] {'y','x'}, dimensions={0} | all-to-all | bytes 262144 | tf_op jit(solution)/shard_map/all_to_all | solution.py:19
  29.1 0.0 copy-done.9
  29.2 0.0 copy-start.2
  29.2 0.0 copy-start.3
  29.2 0.4 shard_map.197
  29.6 26.4 %all_to_all.32.along_z = bf16[16,16,128]{2,1,0:T(8,128)(2,1)S(1)} all-to-all(bf16[16,16,128]{2,1,0:T(8,128)(2,1)S(1)} %bitcast.35), channel_id=1, replica_groups=mesh['z'=16,'c'=2,'y'=4,'x'=4] {'z'}, dimensions={0} | all-to-all | bytes 131072 | tf_op jit(solution)/shard_map/all_to_all | solution.py:19
  56.0 0.2 shard_map.198
  56.2 24.5 %all_to_all.33 = bf16[32,128,128]{2,1,0:T(8,128)(2,1)S(1)} all-to-all(bf16[32,128,128]{2,1,0:T(8,128)(2,1)S(1)} %bitcast.28), channel_id=1, replica_groups=mesh['z'=16,'c'=2,'y'=4,'x'=4] {'c','y','x'}, dimensions={0} | all-to-all | bytes 2097152 | tf_op jit(solution)/shard_map/all_to_all | solution.py:19
  80.8 1.3 %shard_map.199 = (bf16[2,16,128,128]{3,2,1,0:T(8,128)(2,1)S(1)}, f32[64,64,64]{2,1,0:T(8,128)}) custom-call(bf16[2,16,128,128]{3,2,1,0:T(8,128)(2,1)S(1)} %bitcast.30, f32[1,2048]{1,0:T(1,128)S(1)} %bitcast.37, bf16[2048,256]{1,0:T(8,128)(2,1)S(1)} %bitcast.32, bf16[2048,256]{1,0:T(8,128)(2,1)S(1)} %bitcast.33, bf16[256,2048]{1,0:T(8,128)(2,1)S(1)} %bitcast.34, ...), custom_call_target="tpu_custom_call" | custom-call | flops 1073741824 | bytes 1048576 | tf_op jit(solution)/shard_map/pallas_call | solution.py:33
  82.1 0.0 copy-start.15
  82.1 20.8 %all_to_all.34 = bf16[32,128,128]{2,1,0:T(8,128)(2,1)S(1)} all-to-all(bf16[32,128,128]{2,1,0:T(8,128)(2,1)S(1)} %bitcast.31), channel_id=1, replica_groups=mesh['z'=16,'c'=2,'y'=4,'x'=4] {'c','y','x'}, dimensions={0} | all-to-all | bytes 2097152 | tf_op jit(solution)/shard_map/all_to_all | solution.py:19
  102.9 0.1 shard_map.200
  103.0 14.3 %all_to_all.35 = bf16[16,16,128]{2,1,0:T(8,128)(2,1)S(1)} all-to-all(bf16[16,16,128]{2,1,0:T(8,128)(2,1)S(1)} %shard_map.200), channel_id=1, replica_groups=mesh['z'=16,'c'=2,'y'=4,'x'=4] {'z'}, dimensions={0} | all-to-all | bytes 131072 | tf_op jit(solution)/shard_map/all_to_all | solution.py:19
  117.4 0.0 copy-done.15
  117.4 0.8 shard_map.201
  (16 shorter events, 0.0 us)
Async XLA Ops:
  0.6 1.3 %copy-start.12 = (bf16[64,128]{1,0:T(8,128)(2,1)S(1)}, bf16[64,128]{1,0:T(8,128)(2,1)}, u32[]{:S(2)}) copy-start(bf16[64,128]{1,0:T(8,128)(2,1)} %tokens.1) | copy-start | bytes 49156
  2.0 15.4 %copy-start.4 = (f32[64,1,64,64]{3,2,1,0:T(8,128)S(1)}, f32[64,1,64,64]{3,2,1,0:T(8,128)}, u32[]{:S(2)}) copy-start(f32[64,1,64,64]{3,2,1,0:T(8,128)} %param.20) | copy-start | bytes 3145732
  2.0 15.3 %copy-start.5 = (bf16[2048,64]{0,1:T(8,128)(2,1)S(1)}, bf16[2048,64]{0,1:T(8,128)(2,1)}, u32[]{:S(2)}) copy-start(bf16[2048,64]{0,1:T(8,128)(2,1)} %param.23) | copy-start | bytes 786436
  2.0 15.3 %copy-start.6 = (bf16[2048,64]{0,1:T(8,128)(2,1)S(1)}, bf16[2048,64]{0,1:T(8,128)(2,1)}, u32[]{:S(2)}) copy-start(bf16[2048,64]{0,1:T(8,128)(2,1)} %param.24) | copy-start | bytes 786436
  2.0 15.3 %copy-start.7 = (bf16[2048,64]{0,1:T(8,128)(2,1)S(1)}, bf16[2048,64]{0,1:T(8,128)(2,1)}, u32[]{:S(2)}) copy-start(bf16[2048,64]{0,1:T(8,128)(2,1)} %param.25) | copy-start | bytes 786436
  2.0 15.3 %copy-start.8 = (bf16[2048,64]{0,1:T(8,128)(2,1)S(1)}, bf16[2048,64]{0,1:T(8,128)(2,1)}, u32[]{:S(2)}) copy-start(bf16[2048,64]{0,1:T(8,128)(2,1)} %param.26) | copy-start | bytes 786436
  2.0 15.3 %copy-start.10 = (bf16[2048,16]{0,1:T(8,128)(2,1)S(1)}, bf16[2048,16]{0,1:T(8,128)(2,1)}, u32[]{:S(2)}) copy-start(bf16[2048,16]{0,1:T(8,128)(2,1)} %param.27) | copy-start | bytes 196612
  2.0 15.3 %copy-start.11 = (bf16[2048,16]{0,1:T(8,128)(2,1)S(1)}, bf16[2048,16]{0,1:T(8,128)(2,1)}, u32[]{:S(2)}) copy-start(bf16[2048,16]{0,1:T(8,128)(2,1)} %param.28) | copy-start | bytes 196612
  2.0 15.3 %copy-start.13 = (f32[2048]{0:T(1024)S(1)}, f32[2048]{0:T(1024)}, u32[]{:S(2)}) copy-start(f32[2048]{0:T(1024)} %param.21) | copy-start | bytes 24580
  2.1 15.3 %copy-start.16 = (f32[64]{0:T(128)S(1)}, f32[64]{0:T(128)}, u32[]{:S(2)}) copy-start(f32[64]{0:T(128)} %param.31) | copy-start | bytes 772
  17.4 11.8 %copy-start.9 = (bf16[1024,128]{1,0:T(8,128)(2,1)S(1)}, bf16[1024,128]{1,0:T(8,128)(2,1)}, u32[]{:S(2)}) copy-start(bf16[1024,128]{1,0:T(8,128)(2,1)} %w_mix.1) | copy-start | bytes 786436
  17.4 11.7 %copy-start.14 = (s32[64,2]{0,1:T(2,128)S(1)}, s32[64,2]{0,1:T(2,128)}, u32[]{:S(2)}) copy-start(s32[64,2]{0,1:T(2,128)} %param.33) | copy-start | bytes 1540
  29.1 51.6 %copy-start = (bf16[1,2048,256]{2,1,0:T(8,128)(2,1)S(1)}, bf16[1,2048,256]{2,1,0:T(8,128)(2,1)}, u32[]{:S(2)}) copy-start(bf16[1,2048,256]{2,1,0:T(8,128)(2,1)} %param.35) | copy-start | bytes 3145732
  29.2 51.6 %copy-start.1 = (bf16[1,2048,256]{2,1,0:T(8,128)(2,1)S(1)}, bf16[1,2048,256]{2,1,0:T(8,128)(2,1)}, u32[]{:S(2)}) copy-start(bf16[1,2048,256]{2,1,0:T(8,128)(2,1)} %param.36) | copy-start | bytes 3145732
  29.2 51.6 %copy-start.2 = (bf16[1,256,2048]{2,1,0:T(8,128)(2,1)S(1)}, bf16[1,256,2048]{2,1,0:T(8,128)(2,1)}, u32[]{:S(2)}) copy-start(bf16[1,256,2048]{2,1,0:T(8,128)(2,1)} %param.37) | copy-start | bytes 3145732
  29.2 51.6 %copy-start.3 = (f32[2048]{0:T(1024)S(1)}, f32[2048]{0:T(1024)}, u32[]{:S(2)}) copy-start(f32[2048]{0:T(1024)} %param.22) | copy-start | bytes 24580
  82.1 35.3 %copy-start.15 = (f32[64,2]{0,1:T(2,128)S(1)}, f32[64,2]{0,1:T(2,128)}, u32[]{:S(2)}) copy-start(f32[64,2]{0,1:T(2,128)} %param.34) | copy-start | bytes 1540

commit v6 on v5

--- a/solution.py
+++ b/solution.py
@@ -127,20 +127,6 @@
     across = silu(rounded(across))
     query = unit(across[:head_dim]) * head_dim ** (-0.5)
     key = unit(across[head_dim:])
-    both = jnp.concatenate([query, key], axis=0)
-    high = rounded(both)
-    terms = jnp.concatenate([high, both - high], axis=1).astype(BF16)
-    for t in range(0, half, 2):
-        chosen = (owner[...] == t).astype(F32).astype(BF16)
-        repeated = jnp.dot(terms, jnp.concatenate([chosen, chosen], axis=0), preferred_element_type=F32)
-        for step in range(2):
-            row = t + step
-            block = blocks[row]
-            cols = slice(step * 2 * head_dim, (step + 1) * 2 * head_dim)
-            key_pair = repeated[head_dim:, cols]
-            keys[row] = key_pair
-            from_key[row : row + 1, :] = jnp.sum(key_pair * block, axis=0, keepdims=True)
-            from_query[row : row + 1, :] = jnp.sum(repeated[:head_dim, cols] * block, axis=0, keepdims=True)
     overlap = as_column(jnp.sum(query * key, axis=0, keepdims=True))
     overlap = lane_pair(overlap[:half], overlap[half:])
     own = lax.dot_general(rows, jnp.concatenate([wv[...], wg[...]], axis=0), dims, preferred_element_type=F32)
@@ -157,6 +143,20 @@
     soft = jnp.maximum(decay_in, 0.0) + jnp.log1p(jnp.exp(-jnp.abs(decay_in)))
     keep = jnp.exp(-rates_in[0:1, :] * soft)
     beta = 1.0 / (1.0 + jnp.exp(-lane_pair(rates[:half, 1:2], rates[half:, 1:2])))
+    both = jnp.concatenate([query, key], axis=0)
+    high = rounded(both)
+    terms = jnp.concatenate([high, both - high], axis=1).astype(BF16)
+    for t in range(0, half, 2):
+        chosen = (owner[...] == t).astype(F32).astype(BF16)
+        repeated = jnp.dot(terms, jnp.concatenate([chosen, chosen], axis=0), preferred_element_type=F32)
+        for step in range(2):
+            row = t + step
+            block = blocks[row]
+            cols = slice(step * 2 * head_dim, (step + 1) * 2 * head_dim)
+            key_pair = repeated[head_dim:, cols]
+            keys[row] = key_pair
+            from_key[row : row + 1, :] = jnp.sum(key_pair * block, axis=0, keepdims=True)
+            from_query[row : row + 1, :] = jnp.sum(repeated[:head_dim, cols] * block, axis=0, keepdims=True)
     corr = beta * (value - keep * from_key[...])
     reading = keep * from_query[...] + overlap * corr
     squared = reading * reading

time: 119 us -> 118 us (level)
  no operation moved by 1% of the time
where the time goes in v6:
time: 118 us
  blocking collectives  111 us (94%)
  Pallas kernels  4.58 us (4%)
  between operations  2.16 us (2%)
    all_to_all x6, blocking collectives, exchanged(): return lax.all_to_all(blocks, axes, 0, 0, tiled=True)  111 us
    pallas_call x8, Pallas kernels, local_call(): pl.pallas_call(kernel, out_shape=outs, in_specs=[vmem] * len(operands), o...  4.58 us

profile of v6, /device:TPU:1, one launch (start us, length us, event | category | flops | bytes accessed | tf_op | source)
XLA Modules:
  0.0 117.8 jit_solution(9567520440174678524)
XLA Ops:
  0.6 0.0 copy-start.12
  2.0 0.0 copy-start.4
  2.0 0.0 copy-start.5
  2.0 0.0 copy-start.6
  2.0 0.0 copy-start.7
  2.0 0.0 copy-start.8
  2.0 0.0 copy-start.10
  2.0 0.0 copy-start.11
  2.0 0.0 copy-start.13
  2.1 0.0 copy-start.16
  2.1 0.1 shard_map.195
  2.1 15.2 %all_to_all.30.tok = bf16[16,64,128]{2,1,0:T(8,128)(2,1)S(1)} all-to-all(bf16[16,64,128]{2,1,0:T(8,128)(2,1)S(1)} %get-tuple-element.12), channel_id=1, replica_groups=mesh['z'=16,'c'=2,'y'=4,'x'=4] {'y','x'}, dimensions={0} | all-to-all | bytes 524288 | tf_op jit(solution)/shard_map/all_to_all | solution.py:19
  17.3 0.0 copy-done.5
  17.4 0.0 copy-start.9
  17.4 0.0 copy-start.14
  17.4 1.6 %shard_map.196 = (bf16[16,32,128]{2,1,0:T(8,128)(2,1)S(1)}, f32[64,64,64]{2,1,0:T(8,128)S(1)}) custom-call(bf16[16,64,128]{2,1,0:T(8,128)(2,1)S(1)} %all_to_all.30.tok, f32[1,2048]{1,0:T(1,128)S(1)} %bitcast.45, bf16[64,2048]{1,0:T(8,128)(2,1)S(1)} %bitcast.39, bf16[64,2048]{1,0:T(8,128)(2,1)S(1)} %bitcast.40, bf16[64,2048]{1,0:T(8,128)(2,1)S(1)} %bitcast.41, ...), custom_call_target="tpu_custom_call" | custom-call | flops 1073741824 | bytes 1048576 | tf_op jit(solution)/shard_map/pallas_call | solution.py:33
  19.0 9.8 %all_to_all.31.heads = bf16[16,32,128]{2,1,0:T(8,128)(2,1)S(1)} all-to-all(bf16[16,32,128]{2,1,0:T(8,128)(2,1)S(1)} %get-tuple-element.15), channel_id=1, replica_groups=mesh['z'=16,'c'=2,'y'=4,'x'=4] {'y','x'}, dimensions={0} | all-to-all | bytes 262144 | tf_op jit(solution)/shard_map/all_to_all | solution.py:19
  28.8 0.0 copy-done.14
  28.8 0.0 copy-start.2
  28.8 0.0 copy-start.3
  28.8 0.4 shard_map.197
  29.2 26.4 %all_to_all.32.along_z = bf16[16,16,128]{2,1,0:T(8,128)(2,1)S(1)} all-to-all(bf16[16,16,128]{2,1,0:T(8,128)(2,1)S(1)} %bitcast.35), channel_id=1, replica_groups=mesh['z'=16,'c'=2,'y'=4,'x'=4] {'z'}, dimensions={0} | all-to-all | bytes 131072 | tf_op jit(solution)/shard_map/all_to_all | solution.py:19
  55.6 0.2 shard_map.198
  55.8 24.5 %all_to_all.33 = bf16[32,128,128]{2,1,0:T(8,128)(2,1)S(1)} all-to-all(bf16[32,128,128]{2,1,0:T(8,128)(2,1)S(1)} %bitcast.28), channel_id=1, replica_groups=mesh['z'=16,'c'=2,'y'=4,'x'=4] {'c','y','x'}, dimensions={0} | all-to-all | bytes 2097152 | tf_op jit(solution)/shard_map/all_to_all | solution.py:19
  80.3 0.0 copy-done.1
  80.4 1.3 %shard_map.199 = (bf16[2,16,128,128]{3,2,1,0:T(8,128)(2,1)S(1)}, f32[64,64,64]{2,1,0:T(8,128)}) custom-call(bf16[2,16,128,128]{3,2,1,0:T(8,128)(2,1)S(1)} %bitcast.30, f32[1,2048]{1,0:T(1,128)S(1)} %bitcast.37, bf16[2048,256]{1,0:T(8,128)(2,1)S(1)} %bitcast.32, bf16[2048,256]{1,0:T(8,128)(2,1)S(1)} %bitcast.33, bf16[256,2048]{1,0:T(8,128)(2,1)S(1)} %bitcast.34, ...), custom_call_target="tpu_custom_call" | custom-call | flops 1073741824 | bytes 1048576 | tf_op jit(solution)/shard_map/pallas_call | solution.py:33
  81.7 0.0 copy-start.15
  81.7 20.8 %all_to_all.34 = bf16[32,128,128]{2,1,0:T(8,128)(2,1)S(1)} all-to-all(bf16[32,128,128]{2,1,0:T(8,128)(2,1)S(1)} %bitcast.31), channel_id=1, replica_groups=mesh['z'=16,'c'=2,'y'=4,'x'=4] {'c','y','x'}, dimensions={0} | all-to-all | bytes 2097152 | tf_op jit(solution)/shard_map/all_to_all | solution.py:19
  102.5 0.1 shard_map.200
  102.6 14.3 %all_to_all.35 = bf16[16,16,128]{2,1,0:T(8,128)(2,1)S(1)} all-to-all(bf16[16,16,128]{2,1,0:T(8,128)(2,1)S(1)} %shard_map.200), channel_id=1, replica_groups=mesh['z'=16,'c'=2,'y'=4,'x'=4] {'z'}, dimensions={0} | all-to-all | bytes 131072 | tf_op jit(solution)/shard_map/all_to_all | solution.py:19
  117.0 0.0 copy-done.15
  117.0 0.8 shard_map.201
  (16 shorter events, 0.0 us)
Async XLA Ops:
  0.6 1.3 %copy-start.12 = (bf16[64,128]{1,0:T(8,128)(2,1)S(1)}, bf16[64,128]{1,0:T(8,128)(2,1)}, u32[]{:S(2)}) copy-start(bf16[64,128]{1,0:T(8,128)(2,1)} %tokens.1) | copy-start | bytes 49156
  2.0 15.4 %copy-start.4 = (f32[64,1,64,64]{3,2,1,0:T(8,128)S(1)}, f32[64,1,64,64]{3,2,1,0:T(8,128)}, u32[]{:S(2)}) copy-start(f32[64,1,64,64]{3,2,1,0:T(8,128)} %param.20) | copy-start | bytes 3145732
  2.0 15.3 %copy-start.5 = (bf16[2048,64]{0,1:T(8,128)(2,1)S(1)}, bf16[2048,64]{0,1:T(8,128)(2,1)}, u32[]{:S(2)}) copy-start(bf16[2048,64]{0,1:T(8,128)(2,1)} %param.23) | copy-start | bytes 786436
  2.0 15.3 %copy-start.6 = (bf16[2048,64]{0,1:T(8,128)(2,1)S(1)}, bf16[2048,64]{0,1:T(8,128)(2,1)}, u32[]{:S(2)}) copy-start(bf16[2048,64]{0,1:T(8,128)(2,1)} %param.24) | copy-start | bytes 786436
  2.0 15.3 %copy-start.7 = (bf16[2048,64]{0,1:T(8,128)(2,1)S(1)}, bf16[2048,64]{0,1:T(8,128)(2,1)}, u32[]{:S(2)}) copy-start(bf16[2048,64]{0,1:T(8,128)(2,1)} %param.25) | copy-start | bytes 786436
  2.0 15.3 %copy-start.8 = (bf16[2048,64]{0,1:T(8,128)(2,1)S(1)}, bf16[2048,64]{0,1:T(8,128)(2,1)}, u32[]{:S(2)}) copy-start(bf16[2048,64]{0,1:T(8,128)(2,1)} %param.26) | copy-start | bytes 786436
  2.0 15.3 %copy-start.10 = (bf16[2048,16]{0,1:T(8,128)(2,1)S(1)}, bf16[2048,16]{0,1:T(8,128)(2,1)}, u32[]{:S(2)}) copy-start(bf16[2048,16]{0,1:T(8,128)(2,1)} %param.27) | copy-start | bytes 196612
  2.0 15.3 %copy-start.11 = (bf16[2048,16]{0,1:T(8,128)(2,1)S(1)}, bf16[2048,16]{0,1:T(8,128)(2,1)}, u32[]{:S(2)}) copy-start(bf16[2048,16]{0,1:T(8,128)(2,1)} %param.28) | copy-start | bytes 196612
  2.0 15.3 %copy-start.13 = (f32[2048]{0:T(1024)S(1)}, f32[2048]{0:T(1024)}, u32[]{:S(2)}) copy-start(f32[2048]{0:T(1024)} %param.21) | copy-start | bytes 24580
  2.1 15.3 %copy-start.16 = (f32[64]{0:T(128)S(1)}, f32[64]{0:T(128)}, u32[]{:S(2)}) copy-start(f32[64]{0:T(128)} %param.31) | copy-start | bytes 772
  17.4 11.4 %copy-start.9 = (bf16[1024,128]{1,0:T(8,128)(2,1)S(1)}, bf16[1024,128]{1,0:T(8,128)(2,1)}, u32[]{:S(2)}) copy-start(bf16[1024,128]{1,0:T(8,128)(2,1)} %w_mix.1) | copy-start | bytes 786436
  17.4 11.4 %copy-start.14 = (s32[64,2]{0,1:T(2,128)S(1)}, s32[64,2]{0,1:T(2,128)}, u32[]{:S(2)}) copy-start(s32[64,2]{0,1:T(2,128)} %param.33) | copy-start | bytes 1540
  28.8 51.6 %copy-start = (bf16[1,2048,256]{2,1,0:T(8,128)(2,1)S(1)}, bf16[1,2048,256]{2,1,0:T(8,128)(2,1)}, u32[]{:S(2)}) copy-start(bf16[1,2048,256]{2,1,0:T(8,128)(2,1)} %param.35) | copy-start | bytes 3145732
  28.8 51.6 %copy-start.1 = (bf16[1,2048,256]{2,1,0:T(8,128)(2,1)S(1)}, bf16[1,2048,256]{2,1,0:T(8,128)(2,1)}, u32[]{:S(2)}) copy-start(bf16[1,2048,256]{2,1,0:T(8,128)(2,1)} %param.36) | copy-start | bytes 3145732
  28.8 51.6 %copy-start.2 = (bf16[1,256,2048]{2,1,0:T(8,128)(2,1)S(1)}, bf16[1,256,2048]{2,1,0:T(8,128)(2,1)}, u32[]{:S(2)}) copy-start(bf16[1,256,2048]{2,1,0:T(8,128)(2,1)} %param.37) | copy-start | bytes 3145732
  28.8 51.6 %copy-start.3 = (f32[2048]{0:T(1024)S(1)}, f32[2048]{0:T(1024)}, u32[]{:S(2)}) copy-start(f32[2048]{0:T(1024)} %param.22) | copy-start | bytes 24580
  81.7 35.3 %copy-start.15 = (f32[64,2]{0,1:T(2,128)S(1)}, f32[64,2]{0,1:T(2,128)}, u32[]{:S(2)}) copy-start(f32[64,2]{0,1:T(2,128)} %param.34) | copy-start | bytes 1540
